TPU v7x, 512 devices: a whole 4x8x8 slice. The times are simulated.
512 devices in a mesh: ep: 32 (over z, x), tp: 16 (over y, core).
Axes of the slice: x: 4, y: 8, z: 8, core: 2. Of those that a mesh axis runs over, the one named last changes fastest.
Arguments:
- q_in: bfloat16 [16384, 1024], P('ep', 'tp'), may hold values from -6 to 6
- k_in: bfloat16 [16384, 256], P('ep'), may hold values from -6 to 6
- v_in: bfloat16 [16384, 256], P('ep'), may hold values from -6 to 6
- q_gain: float32 [64], replicated, may hold values from 0.1 to 1.9
- k_gain: float32 [64], replicated, may hold values from 0.1 to 1.9
- w_out: bfloat16 [1024, 2048], P('tp'), may hold values from -0.1875 to 0.1875
- post_gain: float32 [2048], replicated, may hold values from 0.1 to 1.9
- moe_in: bfloat16 [4096, 2048], P('ep'), may hold values from -6 to 6
- routes: int32 [4096, 2], P('ep'), may hold values from 0 to 31, all different within a row; in each aligned block of 128 rows (0 to 127, 128 to 255, ...) at most 12 rows name the same one
- route_logits: float32 [4096, 2], P('ep'), may hold values from -6 to 6
- pre_gain: float32 [2048], replicated, may hold values from 0.1 to 1.9
- w_gate: bfloat16 [32, 2048, 4096], P('ep', None, 'tp'), may hold values from -0.125 to 0.125
- w_up: bfloat16 [32, 2048, 4096], P('ep', None, 'tp'), may hold values from -0.125 to 0.125
- w_down: bfloat16 [32, 4096, 2048], P('ep', 'tp'), may hold values from -0.125 to 0.125
Outputs:
- attn_out: bfloat16 [16384, 2048], P(('ep', 'tp'))
- moe_out: bfloat16 [4096, 2048], P('ep', 'tp')
Inputs may be any that keep to these rules, and one draw needn't show every extreme that they name: `routes`: each row names 2 different experts. Among the rows of one index of ep no expert is named by more than 12 rows, a bound that some block reaches of them.
All inputs are finite; a program needn't handle non-finite values.
Results may differ from a plain program's by a relative error of at most 0.018.
Values may be sent and summed in bfloat16 or wider, within the bound.
A program may use at most 64 MiB of HBM per device.

v0:
```python
import jax
import jax.numpy as jnp
from jax import lax
from jax.sharding import Mesh
from jax.sharding import PartitionSpec as P

GRID_W = 128
EP = ("ep_0", "ep_1")
EP_TP = ("ep_0", "ep_1", "tp")


EPSILON = 1e-06
ROPE_BASE = 10000.0


def in_order(blocks, dim):
    blocks = jnp.moveaxis(blocks, 0, dim)
    shape = blocks.shape
    return blocks.reshape(*shape[:dim], shape[dim] * shape[dim + 1], *shape[dim + 2 :])


def copy_for_each(array, axis):
    copies = jnp.broadcast_to(array, (lax.axis_size(axis), *array.shape))
    return lax.all_to_all(copies, axis, split_axis=0, concat_axis=0, tiled=True)


def gathered_copies(array, axis, dim):
    return in_order(copy_for_each(array, axis), dim)


def cut_along(array, dim, size):
    before, after = (array.shape[:dim], array.shape[dim + 1 :])
    return jnp.moveaxis(array.reshape(*before, size, -1, *after), dim, 0)


def turned_blocks(blocks, axes, turns):
    shape = [lax.axis_size(a) for a in axes]
    blocks = blocks.reshape(*shape, *blocks.shape[1:])
    for k in turns:
        blocks = lax.all_to_all(blocks, axes[k], split_axis=k, concat_axis=k, tiled=True)
    return blocks.reshape(-1, *blocks.shape[len(axes) :])


def one_axis_at_a_time(array, axes, turns, split_dim, concat_dim):
    blocks = cut_along(array, split_dim, lax.axis_size(axes))
    return in_order(turned_blocks(blocks, axes, turns), concat_dim)


def head_norm(values, gain):
    return values * lax.rsqrt(jnp.mean(values * values, axis=-1, keepdims=True) + EPSILON) * gain


def rotate_half(values, angles):
    quarter = angles.shape[-1]
    first_part = values[..., :quarter]
    second_part = values[..., quarter:]
    cosine = jnp.cos(angles)[:, None, :]
    sine_part = jnp.sin(angles)[:, None, :]
    return jnp.concatenate(
        [
            first_part * cosine - second_part * sine_part,
            second_part * cosine + first_part * sine_part,
        ],
        axis=-1,
    )


def grid_rotary(values, offset):
    row_count = values.shape[0]
    head_width = values.shape[-1]
    quarter = head_width // 4
    half_width = head_width // 2
    position = offset + jnp.arange(row_count, dtype=jnp.int32)
    grid_row = (position // GRID_W).astype(jnp.float32)
    grid_col = (position % GRID_W).astype(jnp.float32)
    inverse = ROPE_BASE ** (-jnp.arange(quarter, dtype=jnp.float32) / quarter)
    return jnp.concatenate(
        [
            rotate_half(values[..., :half_width], grid_row[:, None] * inverse[None, :]),
            rotate_half(values[..., half_width:], grid_col[:, None] * inverse[None, :]),
        ],
        axis=-1,
    )


def slot_table(route_rows, expert_count, capacity):
    token_count, top_count = route_rows.shape
    flat_routes = route_rows.reshape(-1)
    one_hot = (flat_routes[:, None] == jnp.arange(expert_count, dtype=jnp.int32)[None, :]).astype(
        jnp.int32
    )
    ranked = jnp.sum((jnp.cumsum(one_hot, axis=0) - 1) * one_hot, axis=1)
    placed = flat_routes * capacity + ranked
    slot_owner = jnp.full((expert_count * capacity,), token_count * top_count, dtype=jnp.int32)
    slot_owner = slot_owner.at[placed].set(jnp.arange(token_count * top_count, dtype=jnp.int32))
    return (slot_owner, placed)


def mixer_half(q_in, k_in, v_in, q_gain, k_gain, w_out, post_gain):
    head_size = q_gain.shape[0]
    row_count = q_in.shape[0]
    local_heads = q_in.shape[1] // head_size
    kv_count = k_in.shape[1] // head_size
    tp_count = lax.axis_size("tp")
    repeat = local_heads * tp_count // kv_count
    offset = lax.axis_index(EP) * row_count
    queries = head_norm(q_in.astype(jnp.float32).reshape(row_count, local_heads, head_size), q_gain)
    queries = grid_rotary(queries, offset).astype(jnp.bfloat16)
    query_rows = jnp.transpose(queries, (1, 0, 2)).reshape(local_heads * row_count, head_size)
    kv_index = lax.axis_index("tp") * local_heads // repeat
    own_keys = lax.dynamic_slice_in_dim(k_in, kv_index * head_size, head_size, 1)
    own_values = lax.dynamic_slice_in_dim(v_in, kv_index * head_size, head_size, 1)
    own_keys = head_norm(own_keys.astype(jnp.float32)[:, None, :], k_gain)
    own_keys = grid_rotary(own_keys, offset)[:, 0, :].astype(jnp.bfloat16)
    paired = jnp.concatenate([own_keys, own_values], axis=1)
    scale_factor = head_size ** (-0.5)

    def attend_block(running, key_block):
        block_keys = key_block[:, :head_size]
        block_values = key_block[:, head_size:]
        scores = (
            jnp.einsum("qd,kd->qk", query_rows, block_keys, preferred_element_type=jnp.float32)
            * scale_factor
        )
        weights = jnp.exp(scores)
        numer = running[0] + jnp.dot(
            weights.astype(jnp.bfloat16), block_values, preferred_element_type=jnp.float32
        )
        return (numer, running[1] + jnp.sum(weights, axis=1))

    zero_init = (
        jnp.zeros((local_heads * row_count, head_size), jnp.float32),
        jnp.zeros((local_heads * row_count,), jnp.float32),
    )
    running = zero_init
    gathered_piece = lax.all_gather(paired, EP, axis=0, tiled=True)
    piece_rows = gathered_piece.shape[0]
    blocks = gathered_piece.reshape(piece_rows // 512, 512, gathered_piece.shape[1])

    def scan_block(partial_value, key_block):
        return (attend_block(partial_value, key_block), None)

    running, unused = lax.scan(scan_block, running, blocks)
    numer, denom = running
    head_out = (numer / denom[:, None]).astype(jnp.bfloat16)
    head_out = jnp.transpose(head_out.reshape(local_heads, row_count, head_size), (1, 0, 2))
    head_out = head_out.reshape(row_count, local_heads * head_size)
    mixed = lax.psum_scatter(
        jnp.dot(head_out, w_out, preferred_element_type=jnp.float32).astype(jnp.bfloat16),
        "tp",
        scatter_dimension=0,
        tiled=True,
    ).astype(jnp.float32)
    return head_norm(mixed, post_gain).astype(jnp.bfloat16)


def experts_half(moe_in, routes, route_logits, pre_gain, w_gate, w_up, w_down):
    token_count, top_count = routes.shape
    model_width = moe_in.shape[1]
    expert_count = lax.axis_size(EP)
    capacity = max(2, 3 * top_count * token_count // (2 * expert_count))
    tp_count = lax.axis_size("tp")
    slice_width = model_width // tp_count
    normed = head_norm(moe_in.astype(jnp.float32), pre_gain).astype(jnp.bfloat16)
    slot_owner, placed = slot_table(routes, expert_count, capacity)
    padded = jnp.concatenate([normed, jnp.zeros((1, model_width), jnp.bfloat16)], axis=0)
    outgoing = padded[slot_owner // top_count].reshape(expert_count, capacity, model_width)
    own_slice = lax.dynamic_slice_in_dim(
        outgoing, lax.axis_index("tp") * slice_width, slice_width, 2
    )
    arrived = lax.all_to_all(own_slice, EP, split_axis=0, concat_axis=0, tiled=True)
    arrived = arrived.reshape(expert_count * capacity, slice_width)
    gathered_piece = gathered_copies(arrived, "tp", 1)
    gate_rows = w_gate[0]
    up_rows = w_up[0]
    gate_pre = jnp.dot(gathered_piece, gate_rows, preferred_element_type=jnp.float32)
    up_pre = jnp.dot(gathered_piece, up_rows, preferred_element_type=jnp.float32)
    hidden = (jax.nn.silu(gate_pre) * up_pre).astype(jnp.bfloat16)
    partial_out = jnp.dot(hidden, w_down[0], preferred_element_type=jnp.float32)
    partial_out = partial_out.reshape(expert_count, capacity, model_width)
    summed = lax.psum_scatter(
        partial_out.astype(jnp.bfloat16), "tp", scatter_dimension=2, tiled=True
    )
    returned = one_axis_at_a_time(summed, EP, (0, 1), 0, 0)
    returned = returned.reshape(expert_count * capacity, slice_width)
    copies = returned[placed].reshape(token_count, top_count, slice_width).astype(jnp.float32)
    route_weight = jax.nn.softmax(route_logits, axis=-1)
    return jnp.sum(route_weight[..., None] * copies, axis=1).astype(jnp.bfloat16)


def per_device(
    q_in,
    k_in,
    v_in,
    q_gain,
    k_gain,
    w_out,
    post_gain,
    moe_in,
    routes,
    route_logits,
    pre_gain,
    w_gate,
    w_up,
    w_down,
):
    attn_out = mixer_half(q_in, k_in, v_in, q_gain, k_gain, w_out, post_gain)
    moe_out = experts_half(moe_in, routes, route_logits, pre_gain, w_gate, w_up, w_down)
    return (attn_out, moe_out)


def solution(mesh):
    finer = Mesh(mesh.devices.reshape(8, 4, mesh.shape["tp"]), ("ep_0", "ep_1", "tp"))
    in_specs = (
        P(EP, "tp"),
        P(EP, None),
        P(EP, None),
        P(),
        P(),
        P("tp", None),
        P(),
        P(EP, None),
        P(EP, None),
        P(EP, None),
        P(),
        P(EP, None, "tp"),
        P(EP, None, "tp"),
        P(EP, "tp", None),
    )
    out_specs = (P(EP_TP, None), P(EP, "tp"))
    return jax.shard_map(
        per_device, mesh=finer, in_specs=in_specs, out_specs=out_specs, check_vma=False
    )
```

profile of v0, /device:TPU:1, one launch (start us, length us, event | category | flops | bytes accessed | tf_op | source)
XLA Modules:
  0.0 242.3 jit_solution(13532748336248909430)
XLA Ops:
  8.1 1.3 constant_dynamic-slice_fusion.1
  11.3 0.9 fusion.21
  14.9 1.4 scatter_custom_fusion
  16.8 2.5 %gather_fusion = bf16[384,2048]{1,0:T(8,128)(2,1)S(1)} fusion(bf16[129,2048]{1,0:T(8,128)(2,1)S(1)} %concatenate.32, s32[1024]{0:T(1024)S(1)} %pad_clamp_fusion.1), kind=kCustom, calls=%fused_computation | custom fusion | bytes 3147264 | tf_op jit(solution)/shard_map/gather | solution.py:167
  19.3 1.5 reshape.360
  21.7 24.3 %all_to_all.20 = bf16[32,12,128]{2,1,0:T(8,128)(2,1)S(1)} all-to-all(bf16[32,12,128]{2,1,0:T(8,128)(2,1)S(1)} %constant_dynamic-slice_fusion), channel_id=1, replica_groups=mesh['ep_0'=8,'ep_1'=4,'tp'=16] {'ep_0','ep_1'}, dimensions={0} | all-to-all | bytes 196608 | tf_op jit(solution)/shard_map/all_to_all | solution.py:171
  46.1 1.4 broadcast_in_dim.14
  47.5 8.8 %all-to-all-start.1 = ((bf16[16,384,128]{1,2,0:T(8,128)(2,1)}), bf16[16,384,128]{1,2,0:T(8,128)(2,1)S(1)}, u32[]{:S(2)}, u32[]{:S(2)}) async-start(bf16[16,384,128]{1,2,0:T(8,128)(2,1)} %broadcast_in_dim.14), calls=%async_computation.2 | async-start | bytes 3145728 | tf_op jit(solution)/shard_map/all_to_all | solution.py:24
  56.5 38.3 %all-to-all-done.1 = bf16[16,384,128]{1,2,0:T(8,128)(2,1)S(1)} async-done(((bf16[16,384,128]{1,2,0:T(8,128)(2,1)}), bf16[16,384,128]{1,2,0:T(8,128)(2,1)S(1)}, u32[]{:S(2)}, u32[]{:S(2)}) %all-to-all-start.1) | async-done | bytes 1572896 | tf_op jit(solution)/shard_map/all_to_all | solution.py:24
  94.8 1.9 fusion.10
  98.1 8.5 %copy.55 = bf16[32,12,2048]{0,1,2:T(8,128)(2,1)} copy(bf16[32,12,2048]{2,0,1:T(8,128)(2,1)S(1)} %convolution_convert_fusion.1) | data formatting | bytes 3145728
  106.6 10.3 %reshape.390 = bf16[2048,384]{1,0:T(8,128)(2,1)} reshape(bf16[2048,12,32]{2,1,0:T(8,128)(2,1)} %bitcast.66) | data formatting | bytes 3145728
  117.0 6.4 %copy.54 = bf16[16384,128]{1,0:T(8,128)(2,1)} copy(bf16[16384,128]{0,1:T(8,128)(2,1)} %all-gather.2.cloned.1.call-done) | data formatting | bytes 8388608
  123.4 52.3 %while.13 = (s32[]{:T(128)}, f32[512,64]{0,1:T(8,128)S(1)}, f32[512]{0:T(512)S(1)}, bf16[32,512,128]{2,1,0:T(8,128)(2,1)}, bf16[512,64]{1,0:T(8,128)(2,1)S(1)}, /*index=5*/s32[]{:T(128)}, s32[]{:T(128)}) while((s32[]{:T(128)}, f32[512,64]{0,1:T(8,128)S(1)}, f32[512]{0:T(512)S(1)}, bf16[32,512,128]{2,1,0:T(8,128)(2,1)}, ...), condition=%wide.region_4.5_spmd.clone, body=%wide.region_2.4_spmd.clone.sunk | while | flops 67961344 | bytes 1908828 | solution.py:143
  123.4 1.0 dynamic-slice_bitcast_fusion.2
  125.1 0.9 dynamic-slice_bitcast_fusion.2
  128.4 0.9 dynamic-slice_bitcast_fusion.2
  136.6 0.9 dynamic-slice_bitcast_fusion.2
  139.8 0.9 dynamic-slice_bitcast_fusion.2
  143.1 0.9 dynamic-slice_bitcast_fusion.2
  146.4 0.9 dynamic-slice_bitcast_fusion.2
  161.1 0.9 dynamic-slice_bitcast_fusion.2
  164.3 0.9 dynamic-slice_bitcast_fusion.2
  175.8 2.1 convolution_convert_fusion
  178.6 1.3 reshape.391
  180.9 3.4 %all-to-all-start.2 = ((bf16[8,4,1,12,128]{4,1,3,2,0:T(4,128)(2,1)}), bf16[8,4,1,12,128]{4,1,3,2,0:T(4,128)(2,1)S(1)}, u32[]{:S(2)}, u32[]{:S(2)}) async-start(bf16[8,4,1,12,128]{4,1,3,2,0:T(4,128)(2,1)} %copy.51), calls=%async_computation.3 | async-start | bytes 196608 | tf_op jit(solution)/shard_map/all_to_all | solution.py:40
  184.4 8.5 %all-to-all-done.2 = bf16[8,4,1,12,128]{4,1,3,2,0:T(4,128)(2,1)S(1)} async-done(((bf16[8,4,1,12,128]{4,1,3,2,0:T(4,128)(2,1)}), bf16[8,4,1,12,128]{4,1,3,2,0:T(4,128)(2,1)S(1)}, u32[]{:S(2)}, u32[]{:S(2)}) %all-to-all-start.2) | async-done | bytes 98336 | tf_op jit(solution)/shard_map/all_to_all | solution.py:40
  193.6 3.3 %all-to-all-start.3 = ((bf16[8,4,1,12,128]{4,0,3,2,1:T(8,128)(2,1)}), bf16[8,4,1,12,128]{4,0,3,2,1:T(8,128)(2,1)S(1)}, u32[]{:S(2)}, u32[]{:S(2)}) async-start(bf16[8,4,1,12,128]{4,0,3,2,1:T(8,128)(2,1)} %copy.52), calls=%async_computation.4 | async-start | bytes 196608 | tf_op jit(solution)/shard_map/all_to_all | solution.py:40
  197.0 4.6 %all-to-all-done.3 = bf16[8,4,1,12,128]{4,0,3,2,1:T(8,128)(2,1)S(1)} async-done(((bf16[8,4,1,12,128]{4,0,3,2,1:T(8,128)(2,1)}), bf16[8,4,1,12,128]{4,0,3,2,1:T(8,128)(2,1)S(1)}, u32[]{:S(2)}, u32[]{:S(2)}) %all-to-all-start.3) | async-done | bytes 98336 | tf_op jit(solution)/shard_map/all_to_all | solution.py:40
  203.3 28.8 %reduce-scatter.5.cloned.1.call-done = bf16[32,2048]{1,0:T(8,128)(2,1)} async-done(((bf16[512,2048]{1,0:T(8,128)(2,1)}), bf16[32,2048]{1,0:T(8,128)(2,1)}) %reduce-scatter.5.cloned.1.call-update) | async-done | bytes 131088 | tf_op jit(solution)/shard_map/reduce_scatter | solution.py:148
  232.1 1.0 fusion.12
  233.2 1.7 fusion.14
  (198 shorter events, 54.7 us)
Async XLA Ops:
  8.0 89.5 %copy-start = (bf16[1,256,2048]{2,1,0:T(8,128)(2,1)S(1)}, bf16[1,256,2048]{2,1,0:T(8,128)(2,1)}, u32[]{:S(2)}) copy-start(bf16[1,256,2048]{2,1,0:T(8,128)(2,1)} %param.29) | copy-start | bytes 3145732
  8.0 5.3 %copy-start.6 = (s32[128,2]{0,1:T(2,128)S(1)}, s32[128,2]{0,1:T(2,128)}, u32[]{:S(2)}) copy-start(s32[128,2]{0,1:T(2,128)} %param.24) | copy-start | bytes 3076
  8.0 8.3 %copy-start.1 = (bf16[128,2048]{1,0:T(8,128)(2,1)S(1)}, bf16[128,2048]{1,0:T(8,128)(2,1)}, u32[]{:S(2)}) copy-start(bf16[128,2048]{1,0:T(8,128)(2,1)} %param.23) | copy-start | bytes 1572868
  8.0 109.0 %all-gather.2.cloned.1.call-start = ((), (), s32[]{:S(2)}) async-start(), calls=%async_computation.6 | async-start | bytes 4325376 | tf_op jit(solution)/shard_map/all_gather | solution.py:136
  9.4 7.1 %copy-start.4 = (f32[2048]{0:T(1024)S(1)}, f32[2048]{0:T(1024)}, u32[]{:S(2)}) copy-start(f32[2048]{0:T(1024)} %param.26) | copy-start | bytes 24580
  47.5 47.3 %all-to-all-start.1 = ((bf16[16,384,128]{1,2,0:T(8,128)(2,1)}), bf16[16,384,128]{1,2,0:T(8,128)(2,1)S(1)}, u32[]{:S(2)}, u32[]{:S(2)}) async-start(bf16[16,384,128]{1,2,0:T(8,128)(2,1)} %broadcast_in_dim.14), calls=%async_computation.2 | async-start | bytes 3145728 | tf_op jit(solution)/shard_map/all_to_all | solution.py:24
  56.3 122.3 %reduce-scatter.7.cloned.1.call-start = ((), (), s32[]{:S(2)}) async-start(), calls=%async_computation.8 | async-start | bytes 1671168
  94.8 1.9 copy-start.7
  117.0 115.2 %reduce-scatter.5.cloned.1.call-start = ((), (), s32[]{:S(2)}) async-start(), calls=%async_computation.7 | async-start | bytes 2228224 | tf_op jit(solution)/shard_map/reduce_scatter | solution.py:148
  123.4 52.3 %copy-start.2 = (bf16[64,2048]{1,0:T(8,128)(2,1)S(1)}, bf16[64,2048]{1,0:T(8,128)(2,1)}, u32[]{:S(2)}) copy-start(bf16[64,2048]{1,0:T(8,128)(2,1)} %param.21) | copy-start | bytes 786436
  177.9 0.7 copy-start.3
  179.9 53.3 %copy-start.5 = (f32[2048]{0:T(1024)S(1)}, f32[2048]{0:T(1024)}, u32[]{:S(2)}) copy-start(f32[2048]{0:T(1024)} %param.22) | copy-start | bytes 24580
  180.9 12.0 %all-to-all-start.2 = ((bf16[8,4,1,12,128]{4,1,3,2,0:T(4,128)(2,1)}), bf16[8,4,1,12,128]{4,1,3,2,0:T(4,128)(2,1)S(1)}, u32[]{:S(2)}, u32[]{:S(2)}) async-start(bf16[8,4,1,12,128]{4,1,3,2,0:T(4,128)(2,1)} %copy.51), calls=%async_computation.3 | async-start | bytes 196608 | tf_op jit(solution)/shard_map/all_to_all | solution.py:40
  193.6 7.9 %all-to-all-start.3 = ((bf16[8,4,1,12,128]{4,0,3,2,1:T(8,128)(2,1)}), bf16[8,4,1,12,128]{4,0,3,2,1:T(8,128)(2,1)S(1)}, u32[]{:S(2)}, u32[]{:S(2)}) async-start(bf16[8,4,1,12,128]{4,0,3,2,1:T(8,128)(2,1)} %copy.52), calls=%async_computation.4 | async-start | bytes 196608 | tf_op jit(solution)/shard_map/all_to_all | solution.py:40
Sparse Core Ops, SparseCore 0:
  13.4 92.0 all-gather.1
Sparse Core Ops, SparseCore 1:
  117.0 50.9 reduce-scatter.6
  178.0 54.1 reduce-scatter.4
where the time goes:
time: 245 us; the launch traced here: 242 us
  waiting for transfers between devices  80.3 us (33%)
  local copies, waits for them, and re-layouts  69.7 us (28%)
  matrix products  26.5 us (11%)
  blocking collectives  24.3 us (10%)
  between operations  15.9 us (6%)
  starting transfers between devices  15.6 us (6%)
  other arithmetic  8.79 us (4%)
    all_to_all x1, waiting for transfers between devices, copy_for_each(): return lax.all_to_all(copies, axis, split_axis=0, concat_axis=0, tiled=True)  38.3 us
    squeeze x32, local copies, waits for them, and re-layouts, mixer_half(): running, unused = lax.scan(scan_block, running, blocks)  29.4 us
    reduce_scatter x1, waiting for transfers between devices, mixer_half(): lax.psum_scatter(jnp.dot(head_out, w_out, preferred_element_type=jnp.floa...  28.8 us
    unnamed x25, local copies, waits for them, and re-layouts  28 us
    all_to_all x1, blocking collectives, experts_half(): lax.all_to_all(own_slice, EP, split_axis=0, concat_axis=0, tiled=True)  24.3 us
    all_to_all x2, waiting for transfers between devices, turned_blocks(): lax.all_to_all(blocks, axes[k], split_axis=k, concat_axis=k, tiled=True)  13.1 us
    dot_general x32, matrix products, attend_block(): jnp.einsum('qd,kd->qk', query_rows, block_keys, preferred_element_type=jn...  10.9 us
    dot_general x32, matrix products, attend_block(): jnp.dot(weights.astype(jnp.bfloat16), block_values, preferred_element_typ...  10.5 us
  transfers between devices with their start and end apart: 6, of which 4 were waited for; matrix products, arithmetic and copies ran while one was open for 40% of the time, Pallas kernels for 0%

commit v1 on v0

v1 whole, which is shorter than its diff:
```python
import functools

import jax
import jax.numpy as jnp
from jax import lax
from jax.experimental import pallas as pl
from jax.experimental.pallas import tpu as pltpu
from jax.sharding import Mesh
from jax.sharding import PartitionSpec as P

GRID_W = 128
EPSILON = 1e-06
ROPE_BASE = 10000.0
EP = ("z", "x")
TP = ("y", "c")
ALL = ("z", "x", "y", "c")
NY = 8
ODIM = 80
MESH = pl.DeviceIdType.MESH
BF = jnp.bfloat16
F32 = jnp.float32


def head_norm(values, gain):
    return values * lax.rsqrt(jnp.mean(values * values, axis=-1, keepdims=True) + EPSILON) * gain


def rotate_half(values, angles):
    quarter = angles.shape[-1]
    a = values[..., :quarter]
    b = values[..., quarter:]
    cosine = jnp.cos(angles)
    sine = jnp.sin(angles)
    return jnp.concatenate([a * cosine - b * sine, b * cosine + a * sine], axis=-1)


def grid_rotary(values, offset):
    rows, width = values.shape
    quarter = width // 4
    half = width // 2
    position = offset + jnp.arange(rows, dtype=jnp.int32)
    grid_row = (position // GRID_W).astype(F32)
    grid_col = (position % GRID_W).astype(F32)
    inverse = ROPE_BASE ** (-jnp.arange(quarter, dtype=F32) / quarter)
    return jnp.concatenate(
        [
            rotate_half(values[:, :half], grid_row[:, None] * inverse[None, :]),
            rotate_half(values[:, half:], grid_col[:, None] * inverse[None, :]),
        ],
        axis=-1,
    )


def dot(a, b):
    return jnp.dot(a, b, preferred_element_type=F32)


def dot_t(a, b):
    return lax.dot_general(a, b, (((0,), (0,)), ((), ())), preferred_element_type=F32)


def kernel(
    nz, nx, cap,
    q_ref, kv_ref, og_ref, pf_ref, pb_ref, pg_ref, wg_hbm, wu_hbm, wd_hbm, wo_hbm,
    out_ref, fin_ref,
    kvb, qb, qd, acc, ob, orx, wob, pa, ra,
    zrx, xsb, xb, wg, wu, wd, ga, up, tmp, own, pbuf, prx, psb, rs, ret, rbk, t2, fin,
    lsem, kxs, kxr, rrs, rrr, rls, rlr, qs, qr, ts, tr, wos, wor, as_, ar,
    zs, zr, xs, xr, ys, yr, ds, dr, es, er, ms, mr, vs, vr, us, ur,
):
    z, x, y, c = (lax.axis_index(n) for n in ALL)
    rows = nz * nx * cap
    zb, xbk = nx * cap, nz * cap
    b = lax.rem(y, 2)
    h = y // 2
    m = b * 2 + c
    ysw = y + 1 - 2 * b
    oc = 1 - c
    sgn = 1 - 2 * c

    def yy(k):
        return lax.rem(y + (k + 2 * NY), NY)

    def zz(k):
        return lax.rem(z + (k + nz), nz)

    def xx(k):
        return lax.rem(x + (k + nx), nx)

    sent = []

    def rc(src, dst, ss, rr, dz=None, dx=None, dy=None, dc=None):
        dev = (z if dz is None else dz, x if dx is None else dx, y if dy is None else dy, c if dc is None else dc)
        return pltpu.make_async_remote_copy(src, dst, ss, rr, device_id=dev, device_id_type=MESH)

    def send(*args, **kw):
        copy = rc(*args, **kw)
        copy.start()
        sent.append(copy)

    def local(src, dst, i):
        copy = pltpu.make_async_copy(src, dst, lsem.at[i])
        copy.start()
        return copy

    lwo = local(wo_hbm, wob.at[m], 0)
    lwg = local(wg_hbm, wg, 1)
    lwu = local(wu_hbm, wu, 2)
    lwd = [local(wd_hbm.at[:, k * 256 : (k + 1) * 256], wd.at[k], 3 + k) for k in range(NY)]

    bar = pltpu.get_barrier_semaphore()
    peers = [(zz(k), x, y, c) for k in range(1, nz)]
    peers += [(z, xx(k), y, c) for k in range(1, nx)]
    peers += [(z, x, yy(k), c) for k in (1, -1, 2, -2, 4)]
    peers += [(z, x, y, oc), (z, x, ysw, oc)]
    for peer in peers:
        pl.semaphore_signal(bar, inc=1, device_id=peer, device_id_type=MESH)
    kvb[z, x] = kv_ref[...]
    qb[m] = q_ref[...]
    zrow = pl.multiple_of(z * zb, 16)
    zrx[pl.ds(zrow, zb), :] = og_ref[pl.ds(zrow, zb), :]
    pl.semaphore_wait(bar, len(peers))

    for k in range(1, nx):
        send(kv_ref, kvb.at[z, x], kxs.at[k], kxr.at[k], dx=xx(k))
    for k in range(1, nz):
        to = pl.multiple_of(zz(k) * zb, 16)
        send(og_ref.at[pl.ds(to, zb)], zrx.at[pl.ds(zrow, zb)], zs.at[k], zr.at[k], dz=zz(k))
    send(q_ref, qb.at[m], qs.at[0], qr.at[0], dc=oc)
    send(q_ref, qb.at[m], qs.at[1], qr.at[1], dy=ysw)
    send(q_ref, qb.at[m], qs.at[2], qr.at[2], dy=ysw, dc=oc)

    for j in range(8):
        qd[j] = jnp.zeros((128, 512), BF)
        acc[j] = jnp.zeros((ODIM, 256), F32)

    for k in range(1, nx):
        rc(kv_ref, kvb.at[z, xx(-k)], kxs.at[k], kxr.at[k]).wait_recv()

    def ring(step):
        if step < nz // 2:
            g = kvb.at[zz(-step)]
            send(g, g, rrs.at[step], rrr.at[step], dz=zz(1))
        if step < (nz - 1) // 2:
            g = kvb.at[zz(step)]
            send(g, g, rls.at[step], rlr.at[step], dz=zz(-1))

    def ring_wait(step):
        got = []
        if step < nz // 2:
            g = kvb.at[zz(-step - 1)]
            rc(g, g, rrs.at[step], rrr.at[step]).wait_recv()
            got.append(zz(-step - 1))
        if step < (nz - 1) // 2:
            g = kvb.at[zz(step + 1)]
            rc(g, g, rls.at[step], rlr.at[step]).wait_recv()
            got.append(zz(step + 1))
        return got

    ring(0)

    for k in range(1, nz):
        frm = pl.multiple_of(zz(-k) * zb, 16)
        rc(og_ref.at[pl.ds(0, zb)], zrx.at[pl.ds(frm, zb)], zs.at[k], zr.at[k]).wait_recv()
    xsb[...] = dot(pf_ref[...], zrx[...]).astype(BF)
    cl = pl.multiple_of(c * 128, 128)
    ocl = pl.multiple_of(oc * 128, 128)
    xrow = pl.multiple_of(x * xbk, 16)
    slots = (yy(0), yy(4))
    for i in range(2):
        xb[slots[i], pl.ds(xrow, xbk), pl.ds(cl, 128)] = xsb[pl.ds(xrow, xbk), i * 128 : (i + 1) * 128]
    for k in range(1, nx):
        to = pl.multiple_of(xx(k) * xbk, 16)
        for i in range(2):
            send(
                xsb.at[pl.ds(to, xbk), pl.ds(i * 128, 128)],
                xb.at[slots[i], pl.ds(xrow, xbk), pl.ds(cl, 128)],
                xs.at[i, k], xr.at[i, k], dx=xx(k),
            )

    rc(q_ref, qb.at[b * 2 + oc], qs.at[0], qr.at[0]).wait_recv()
    rc(q_ref, qb.at[(1 - b) * 2 + c], qs.at[1], qr.at[1]).wait_recv()
    rc(q_ref, qb.at[(1 - b) * 2 + oc], qs.at[2], qr.at[2]).wait_recv()
    for mt in range(4):
        for rp in range(2):
            pair = [qb[2 * rp + i, :, mt * 128 : (mt + 1) * 128] for i in range(2)]
            pair = jnp.concatenate(pair, axis=1)
            qd[mt * 2 + rp, 0:64, 0:256] = pair
            qd[mt * 2 + rp, 64:128, 256:512] = pair

    def attend(zi):
        keys = kvb[zi, :, 0:64, :].reshape(nx * 64, 128)
        vals = [kvb[zi, i, 64:128, :] for i in range(nx)]
        vals = jnp.concatenate(vals, axis=1)
        vals = jnp.concatenate([vals, jnp.ones((ODIM - 64, nx * 128), BF)], axis=0)

        def tile(j, carry):
            p = jnp.exp(dot(keys, qd[j])).astype(BF)
            parts = []
            for i in range(nx):
                parts.append(p[i * 64 : (i + 1) * 64, 0:256])
                parts.append(p[i * 64 : (i + 1) * 64, 256:512])
            acc[j] += dot(vals, jnp.concatenate(parts, axis=0))
            return carry

        lax.fori_loop(0, 8, tile, 0)

    attend(z)

    for k in range(1, nx):
        frm = pl.multiple_of(xx(-k) * xbk, 16)
        for i in range(2):
            rc(
                xsb.at[pl.ds(0, xbk), pl.ds(i * 128, 128)],
                xb.at[slots[i], pl.ds(frm, xbk), pl.ds(cl, 128)],
                xs.at[i, k], xr.at[i, k],
            ).wait_recv()

    def half(slot, which):
        return xb.at[slot, :, pl.ds(which, 128)]

    plan = ((1, 0), (1, 4), (-1, 0), (-1, 4), (2, 0), (-2, 0))
    for i, (k, r) in enumerate(plan):
        g = half(yy(r), cl)
        send(g, g, ys.at[i], yr.at[i], dy=yy(k))

    def swap(r):
        g = half(yy(r), cl)
        send(g, g, ds.at[r], dr.at[r], dc=oc)

    swap(0)
    swap(4)
    lwo.wait()
    send(wob.at[m], wob.at[m], wos.at[0], wor.at[0], dc=oc)
    send(wob.at[m], wob.at[m], wos.at[1], wor.at[1], dy=ysw)

    def arrive(i):
        k, r = plan[i]
        g = half(yy(r - k), cl)
        rc(g, g, ys.at[i], yr.at[i]).wait_recv()
        swap((r - k + NY) % NY)

    steps = max(nz // 2, (nz - 1) // 2)
    for step in range(steps):
        got = ring_wait(step)
        ring(step + 1)
        if step == steps - 2:
            for i in range(4):
                arrive(i)
        for zi in got:
            attend(zi)
    if steps < 2:
        for i in range(4):
            arrive(i)
    for i in range(4, 6):
        arrive(i)

    for j in range(8):
        a = acc[j]
        den = a[64:ODIM]
        hi = den.astype(BF)
        lo = (den - hi.astype(F32)).astype(BF)
        first = lax.broadcasted_iota(jnp.int32, (ODIM - 64, 256), 0) == 0
        ob[j, 0:64] = a[0:64].astype(BF)
        ob[j, 64:ODIM] = jnp.where(first, hi.astype(F32), lo.astype(F32)).astype(BF)
    other = wob.at[(1 - b) * 2 + c]
    rc(other, other, wos.at[1], wor.at[1]).wait_recv()
    send(other, other, wos.at[2], wor.at[2], dc=oc)
    members = ((0, y, oc, b * 2 + oc), (1, ysw, c, (1 - b) * 2 + c), (2, ysw, oc, (1 - b) * 2 + oc))
    for i, dy, dc, mm in members:
        send(ob.at[pl.ds(2 * mm, 2)], orx.at[i], ts.at[i], tr.at[i], dy=dy, dc=dc)

    lwg.wait()
    lwu.wait()
    for i, r in enumerate((0, 4, 1, 5, 7, 3, 2, 6)):
        s = yy(r)
        g = half(s, ocl)
        rc(g, g, ds.at[r], dr.at[r]).wait_recv()
        w0 = pl.multiple_of(s * 256, 256)
        gd = dot(xb[s], wg[pl.ds(w0, 256), :])
        ud = dot(xb[s], wu[pl.ds(w0, 256), :])
        if i == 0:
            ga[...] = gd
            up[...] = ud
        else:
            ga[...] += gd
            up[...] += ud
    gate = ga[...]
    hid = (gate / (1.0 + jnp.exp(-gate)) * up[...]).astype(BF)
    for copy in lwd:
        copy.wait()
    order = (4, 3, 5, 1, 7, 2, 6, 0)
    for r in order:
        tmp[r % 2] = dot(hid, wd[yy(r)])
        own[r] = tmp[r % 2, :, pl.ds(cl, 128)]
        pbuf[r] = tmp[r % 2, :, pl.ds(ocl, 128)].astype(BF)
        send(pbuf.at[r], prx.at[r], es.at[r], er.at[r], dc=oc)

    def paired(r):
        rc(pbuf.at[r], prx.at[r], es.at[r], er.at[r]).wait_recv()
        return own[r] + prx[r].astype(F32)

    for r, i, dest in ((4, 0, yy(0 - 2 * sgn)), (3, 1, yy(1)), (5, 2, yy(-1)), (1, 3, yy(1)), (7, 4, yy(-1))):
        psb[r] = paired(r).astype(BF)
        send(psb.at[r], rs.at[i], ms.at[i], mr.at[i], dy=dest)

    def got_rs(i):
        rc(psb.at[0], rs.at[i], ms.at[i], mr.at[i]).wait_recv()
        return rs[i].astype(F32)

    for i, dy, dc, mm in members:
        rc(ob.at[pl.ds(0, 2)], orx.at[i], ts.at[i], tr.at[i]).wait_recv()
    heads = []
    for rp in range(2):
        t = ob[2 * m + rp].astype(F32)
        for i in range(3):
            t += orx[i, rp].astype(F32)
        o = (t[0:64] / (t[64:65] + t[65:66])).astype(BF)
        heads += [o[:, 0:128], o[:, 128:256]]
    hot = jnp.concatenate(heads, axis=0)
    partner = wob.at[b * 2 + oc]
    rc(partner, partner, wos.at[0], wor.at[0]).wait_recv()
    far = wob.at[(1 - b) * 2 + oc]
    rc(far, far, wos.at[2], wor.at[2]).wait_recv()
    for n in range(4):
        part = dot_t(hot, wob[:, :, n * 512 : (n + 1) * 512].reshape(256, 512))
        pa[:, :, n * 512 : (n + 1) * 512] = part.astype(BF).reshape(4, 32, 512)

    far_sum = got_rs(0)
    right = c.astype(F32)
    psb[2] = (paired(2) + got_rs(1) + far_sum * right).astype(BF)
    send(psb.at[2], rs.at[5], ms.at[5], mr.at[5], dy=yy(2))
    psb[6] = (paired(6) + got_rs(2) + far_sum * (1.0 - right)).astype(BF)
    send(psb.at[6], rs.at[6], ms.at[6], mr.at[6], dy=yy(-2))

    for k in range(1, 4):
        send(pa.at[lax.rem(h + k, 4)], ra.at[k - 1], as_.at[k - 1], ar.at[k - 1], dy=yy(2 * k))

    ret[...] = (paired(0) + got_rs(3) + got_rs(4) + got_rs(5) + got_rs(6)).astype(BF)
    rbk[pl.ds(xrow, xbk), :] = ret[pl.ds(xrow, xbk), :]
    for k in range(1, nx):
        to = pl.multiple_of(xx(k) * xbk, 16)
        send(ret.at[pl.ds(to, xbk)], rbk.at[pl.ds(xrow, xbk)], vs.at[k], vr.at[k], dx=xx(k))
    for k in range(1, nx):
        frm = pl.multiple_of(xx(-k) * xbk, 16)
        rc(ret.at[pl.ds(0, xbk)], rbk.at[pl.ds(frm, xbk)], vs.at[k], vr.at[k]).wait_recv()
    t2[...] = dot(pb_ref[...], rbk[...]).astype(BF)
    fin[pl.ds(zrow, zb), :] = t2[pl.ds(zrow, zb), :]
    for k in range(1, nz):
        to = pl.multiple_of(zz(k) * zb, 16)
        send(t2.at[pl.ds(to, zb)], fin.at[pl.ds(zrow, zb)], us.at[k], ur.at[k], dz=zz(k))

    mixed = pa[h].astype(F32)
    for k in range(1, 4):
        rc(pa.at[0], ra.at[k - 1], as_.at[k - 1], ar.at[k - 1]).wait_recv()
        mixed += ra[k - 1].astype(F32)
    scale = lax.rsqrt(jnp.mean(mixed * mixed, axis=1, keepdims=True) + EPSILON)
    out_ref[...] = (mixed * scale * pg_ref[...]).astype(BF)

    for k in range(1, nz):
        frm = pl.multiple_of(zz(-k) * zb, 16)
        rc(t2.at[pl.ds(0, zb)], fin.at[pl.ds(frm, zb)], us.at[k], ur.at[k]).wait_recv()
    fin_ref[...] = fin[...]
    for copy in sent:
        copy.wait_send()


def call(nz, nx, cap, *args):
    rows = nz * nx * cap
    vm = pl.BlockSpec(memory_space=pltpu.VMEM)
    hbm = pl.BlockSpec(memory_space=pl.ANY)
    dma = lambda *n: pltpu.SemaphoreType.DMA(n)
    big = lambda *s: pltpu.VMEM(s, BF)
    wide = lambda *s: pltpu.VMEM(s, F32)
    scratch = [
        big(nz, nx, 128, 128), big(4, 64, 512), big(8, 128, 512), wide(8, ODIM, 256), big(8, ODIM, 256),
        big(3, 2, ODIM, 256), big(4, 64, 2048), big(4, 32, 2048), big(3, 32, 2048),
        big(rows, 256), big(rows, 256), big(NY, rows, 256), big(2048, 256), big(2048, 256), big(NY, 256, 256),
        wide(rows, 256), wide(rows, 256), wide(2, rows, 256), wide(NY, rows, 128), big(NY, rows, 128),
        big(NY, rows, 128), big(NY, rows, 128), big(7, rows, 128), big(rows, 128), big(rows, 128),
        big(rows, 128), big(rows, 128),
        dma(11), dma(nx), dma(nx), dma(nz), dma(nz), dma(nz), dma(nz), dma(3), dma(3), dma(3), dma(3), dma(3), dma(3),
        dma(3), dma(3),
        dma(nz), dma(nz), dma(2, nx), dma(2, nx), dma(6), dma(6), dma(8), dma(8), dma(8), dma(8), dma(7), dma(7),
        dma(nx), dma(nx), dma(nz), dma(nz),
    ]
    return pl.pallas_call(
        functools.partial(kernel, nz, nx, cap),
        out_shape=(jax.ShapeDtypeStruct((32, 2048), BF), jax.ShapeDtypeStruct((rows, 128), BF)),
        in_specs=[vm] * 6 + [hbm] * 4,
        out_specs=(vm, vm),
        scratch_shapes=scratch,
        compiler_params=pltpu.CompilerParams(
            collective_id=0, has_side_effects=True, vmem_limit_bytes=48 * 1024 * 1024
        ),
        name="layer",
    )(*args)


def per_device(
    q_in, k_in, v_in, q_gain, k_gain, w_out, post_gain, moe_in, routes, route_logits, pre_gain, w_gate, w_up, w_down
):
    nz, nx = lax.axis_size("z"), lax.axis_size("x")
    y, c = lax.axis_index("y"), lax.axis_index("c")
    ep = lax.axis_index(EP)
    count, top = routes.shape
    experts = nz * nx
    cap = max(2, 3 * top * count // (2 * experts))
    rows = experts * cap
    offset = ep * 512
    h = y // 2
    m = lax.rem(y, 2) * 2 + c

    q = grid_rotary(head_norm(q_in.astype(F32), q_gain), offset).astype(BF) * BF(0.125)
    q = jnp.transpose(q.reshape(4, 4, 32, 64), (3, 1, 0, 2)).reshape(64, 512)
    k = lax.dynamic_slice(k_in, (m * 128, h * 64), (128, 64)).astype(F32)
    k = grid_rotary(head_norm(k, k_gain), offset + m * 128).astype(BF)
    v = lax.dynamic_slice(v_in, (m * 128, h * 64), (128, 64))
    kv = jnp.concatenate([jnp.concatenate([k[:64], k[64:]], axis=1), v.T], axis=0)

    x32 = moe_in.astype(F32)
    scale = lax.rsqrt(jnp.mean(x32 * x32, axis=-1, keepdims=True) + EPSILON)
    cols = [(lax.rem(y + 4 * i, NY) * 2 + c) * 128 for i in range(2)]
    xs = [lax.dynamic_slice(moe_in, (0, col), (count, 128)).astype(F32) for col in cols]
    gs = [lax.dynamic_slice(pre_gain, (col,), (128,)) for col in cols]
    xn = jnp.concatenate([(v_ * scale * g_).astype(BF) for v_, g_ in zip(xs, gs)], axis=1)
    rt = routes.T
    eid = jnp.arange(experts, dtype=jnp.int32)[:, None]
    hot = [(eid == rt[i][None, :]) for i in range(top)]
    both = (hot[0] | hot[1]).astype(BF)
    tri = (jnp.arange(count)[:, None] < jnp.arange(count)[None, :]).astype(BF)
    rank = dot(both, tri).astype(jnp.int32)
    place = [jnp.sum(jnp.where(hh, rank + cap * eid, 0), axis=0) for hh in hot]
    slot = jnp.arange(rows, dtype=jnp.int32)[:, None]
    sel = [(slot == pp[None, :]) for pp in place]
    og = dot((sel[0] | sel[1]).astype(BF), xn).astype(BF)

    i = jnp.arange(rows, dtype=jnp.int32)
    src = (i % (nz * cap)) // cap * (nx * cap) + i // (nz * cap) * cap + i % cap
    pf = (src[:, None] == i[None, :]).astype(BF)
    pb = (src[None, :] == i[:, None]).astype(BF)

    attn, fin = call(
        nz, nx, cap, q, kv, og, pf, pb, post_gain[None, :], w_gate[0], w_up[0], w_down[0], w_out
    )
    weight = jax.nn.softmax(route_logits, axis=-1)
    moe = sum(weight[:, j : j + 1] * dot_t(sel[j].astype(BF), fin) for j in range(top))
    return attn, moe.astype(BF)


def solution(mesh):
    ny = mesh.shape["tp"] // 2
    nz = 8 if mesh.shape["ep"] % 8 == 0 else 2
    finer = Mesh(mesh.devices.reshape(nz, mesh.shape["ep"] // nz, ny, 2), ALL)
    in_specs = (
        P(EP, TP), P(EP, None), P(EP, None), P(), P(), P(TP, None), P(), P(EP, None), P(EP, None), P(EP, None), P(),
        P(EP, None, TP), P(EP, None, TP), P(EP, TP, None),
    )
    return jax.shard_map(
        per_device, mesh=finer, in_specs=in_specs, out_specs=(P(ALL, None), P(EP, TP)), check_vma=False
    )
```

time: 245 us -> 103 us (0.42)
  waiting for transfers between devices: 80.3 us -> 0 us
  Pallas kernels: 0 us -> 79.6 us
  local copies, waits for them, and re-layouts: 69.7 us -> 12.5 us
  matrix products: 26.5 us -> 1.48 us
  blocking collectives: 24.3 us -> 0 us
  starting transfers between devices: 15.6 us -> 0 us
  between operations: 15.9 us -> 0.96 us
    pallas_call x0 -> x1, Pallas kernels: none -> 79.6 us  [call(): pl.pallas_call(functools.partial(kernel, nz, nx, cap), out_shape=(jax.Sha...]
    all_to_all x3 -> x0, waiting for transfers between devices: 51.5 us -> none  [the longest x1 38.3 us: copy_for_each(): return lax.all_to_all(copies, axis, split_axis=0, concat_axis=0, tiled=True)]
    squeeze x32 -> x0, local copies, waits for them, and re-layouts: 29.4 us -> none  [mixer_half(): running, unused = lax.scan(scan_block, running, blocks)]
    reduce_scatter x1 -> x0, waiting for transfers between devices: 28.8 us -> none  [mixer_half(): lax.psum_scatter(jnp.dot(head_out, w_out, preferred_element_type=jnp.floa...]
    dot_general x68 -> x4, matrix products: 26.5 us -> 1.48 us  [the longest x2 1.13 us: dot_t(): lax.dot_general(a, b, (((0,), (0,)), ((), ())), preferred_element_type=F32)]
    all_to_all x1 -> x0, blocking collectives: 24.3 us -> none  [experts_half(): lax.all_to_all(own_slice, EP, split_axis=0, concat_axis=0, tiled=True)]
    unnamed x25 -> x26, local copies, waits for them, and re-layouts: 28 us -> 4.78 us
    all_to_all x3 -> x0, starting transfers between devices: 15.5 us -> none  [the longest x1 8.81 us: copy_for_each(): return lax.all_to_all(copies, axis, split_axis=0, concat_axis=0, tiled=True)]
  transfers between devices with their start and end apart: 6 -> 0, of which waited for: 4 -> 0; matrix products, arithmetic and copies ran while one was open for 40% -> 0% of each run, Pallas kernels for 0% -> 0%
where the time goes in v1:
time: 103 us; the launch traced here: 102 us
  Pallas kernels  79.6 us (77%)
  local copies, waits for them, and re-layouts  12.5 us (12%)
  other arithmetic  8.02 us (8%)
  matrix products  1.48 us (1%)
    pallas_call x1, Pallas kernels, call(): pl.pallas_call(functools.partial(kernel, nz, nx, cap), out_shape=(jax.Sha...  79.6 us
    concatenate x8, local copies, waits for them, and re-layouts, grid_rotary(): jnp.concatenate([rotate_half(values[:, :half], grid_row[:, None] * invers...  5.82 us
    unnamed x26, local copies, waits for them, and re-layouts  4.78 us

profile of v1, /device:TPU:1, one launch (start us, length us, event | category | flops | bytes accessed | tf_op | source)
XLA Modules:
  0.0 102.5 jit_solution(13038888148931353214)
XLA Ops:
  0.7 1.2 %multiply_reduce_fusion = f32[128]{0:T(128)S(1)} fusion(bf16[128,2048]{1,0:T(8,128)(2,1)} %param.21), kind=kLoop, calls=%fused_computation.7 | loop fusion | flops 786304 | bytes 524800 | tf_op jit(solution)/shard_map/reduce_sum | solution.py:422
  1.9 0.8 fusion.81
  2.7 0.9 multiply_convert_fusion.1
  3.5 0.7 copy-done.9
  4.2 0.2 select_reduce_fusion.1
  4.4 0.2 convolution_convert_fusion.og_ref
  4.6 0.9 fusion.21
  5.6 0.6 copy-done.10
  6.2 0.8 fusion.22
  7.1 0.6 fusion.28
  7.7 0.1 pad_maximum_fusion
  7.8 0.9 dynamic_slice.19
  9.0 0.4 copy-done.11
  9.5 0.3 fusion.47
  9.8 0.1 concatenate.26
  9.9 0.1 copy.27
  10.0 0.1 concatenate.27
  10.2 0.8 copy.28
  10.9 0.7 concatenate.28
  11.7 1.6 %copy.29 = bf16[4,4,32,16]{3,2,0,1:T(8,128)(2,1)} copy(bf16[4,4,32,16]{2,1,0,3:T(4,128)(2,1)} %concatenate.28) | data formatting | bytes 32768 | tf_op jit(solution)/shard_map/concatenate | solution.py:45
  13.3 0.7 concatenate.29
  14.0 1.6 %copy.30 = bf16[4,4,32,16]{3,2,0,1:T(8,128)(2,1)} copy(bf16[4,4,32,16]{2,1,0,3:T(4,128)(2,1)} %concatenate.29) | data formatting | bytes 32768 | tf_op jit(solution)/shard_map/concatenate | solution.py:45
  15.6 1.9 %maximum_multiply_fusion = bf16[4,4,32,64]{3,2,0,1:T(8,128)(2,1)} fusion(bf16[4,4,32,16]{3,2,0,1:T(8,128)(2,1)} %copy.30, bf16[4,4,32,16]{3,2,0,1:T(8,128)(2,1)} %copy.29, bf16[4,4,32,16]{3,2,0,1:T(8,128)(2,1)} %copy.28, bf16[4,4,32,16]{3,2,0,1:T(8,128)(2,1)S(1)} %copy.27), kind=kLoop, calls=%fused_computation.19 | loop fusion | flops 327680 | bytes 131072 | tf_op jit(solution)/shard_map/mul | solution.py:414
  17.5 1.0 copy.34.q_ref
  18.5 0.2 fusion.4
  18.8 0.9 copy-done.3
  19.7 79.6 %layer.1 = (bf16[32,2048]{1,0:T(8,128)(2,1)S(1)}, bf16[384,128]{1,0:T(8,128)(2,1)S(1)}) custom-call(bf16[64,512]{1,0:T(8,128)(2,1)S(1)} %copy.34.q_ref, bf16[128,128]{1,0:T(8,128)(2,1)S(1)} %pad_maximum_fusion.1.kv_ref, bf16[384,256]{1,0:T(8,128)(2,1)S(1)} %convolution_convert_fusion.og_ref, bf16[384,384]{1,0:T(8,128)(2,1)S(1)} %get-tuple-element.27.pf_ref, ...), custom_call_target="tpu_custom_call" | custom-call | tf_op jit(solution)/shard_map/layer/pallas_call | solution.py:387
  99.3 0.6 copy-done.4
  99.9 0.7 copy-done.8
  100.7 0.3 convolution_multiply_fusion.1
  100.9 0.9 fusion.1
  101.8 0.7 copy.37
  (35 shorter events, 0.5 us)
Async XLA Ops:
  3.5 0.7 copy-start.9
  5.6 0.7 copy-start.10
  7.8 1.1 %copy-start.7 = (bf16[512,64]{0,1:T(8,128)(2,1)S(1)}, bf16[512,64]{0,1:T(8,128)(2,1)}, u32[]{:S(2)}) copy-start(bf16[512,64]{0,1:T(8,128)(2,1)} %param.14) | copy-start | bytes 196612
  7.8 10.9 %copy-start.6 = (f32[2048]{0:T(1024)S(1)}, f32[2048]{0:T(1024)}, u32[]{:S(2)}) copy-start(f32[2048]{0:T(1024)} %param.20) | copy-start | bytes 24580
  8.7 0.7 copy-start.11
  8.8 9.9 %copy-start.2 = (bf16[1,256,2048]{2,1,0:T(8,128)(2,1)S(1)}, bf16[1,256,2048]{2,1,0:T(8,128)(2,1)}, u32[]{:S(2)}) copy-start(bf16[1,256,2048]{2,1,0:T(8,128)(2,1)} %param.27) | copy-start | bytes 3145732
  10.1 8.6 %copy-start.1 = (bf16[1,2048,256]{2,1,0:T(8,128)(2,1)S(1)}, bf16[1,2048,256]{2,1,0:T(8,128)(2,1)}, u32[]{:S(2)}) copy-start(bf16[1,2048,256]{2,1,0:T(8,128)(2,1)} %param.26) | copy-start | bytes 3145732
  10.9 7.8 %copy-start = (bf16[1,2048,256]{2,1,0:T(8,128)(2,1)S(1)}, bf16[1,2048,256]{2,1,0:T(8,128)(2,1)}, u32[]{:S(2)}) copy-start(bf16[1,2048,256]{2,1,0:T(8,128)(2,1)} %param.25) | copy-start | bytes 3145732
  18.7 1.0 copy-start.3
  99.3 0.7 copy-start.4
  99.9 0.7 copy-start.8
  100.9 0.9 copy-start.5

commit v2 on v1

--- a/solution.py
+++ b/solution.py
@@ -2,6 +2,7 @@
 
 import jax
 import jax.numpy as jnp
+import numpy as np
 from jax import lax
 from jax.experimental import pallas as pl
 from jax.experimental.pallas import tpu as pltpu
@@ -21,34 +22,12 @@
 F32 = jnp.float32
 
 
-def head_norm(values, gain):
-    return values * lax.rsqrt(jnp.mean(values * values, axis=-1, keepdims=True) + EPSILON) * gain
-
-
-def rotate_half(values, angles):
-    quarter = angles.shape[-1]
-    a = values[..., :quarter]
-    b = values[..., quarter:]
-    cosine = jnp.cos(angles)
-    sine = jnp.sin(angles)
-    return jnp.concatenate([a * cosine - b * sine, b * cosine + a * sine], axis=-1)
-
-
-def grid_rotary(values, offset):
-    rows, width = values.shape
-    quarter = width // 4
-    half = width // 2
-    position = offset + jnp.arange(rows, dtype=jnp.int32)
-    grid_row = (position // GRID_W).astype(F32)
-    grid_col = (position % GRID_W).astype(F32)
-    inverse = ROPE_BASE ** (-jnp.arange(quarter, dtype=F32) / quarter)
-    return jnp.concatenate(
-        [
-            rotate_half(values[:, :half], grid_row[:, None] * inverse[None, :]),
-            rotate_half(values[:, half:], grid_col[:, None] * inverse[None, :]),
-        ],
-        axis=-1,
-    )
+def angle_table():
+    lane = np.arange(128)
+    inverse = np.float32(ROPE_BASE) ** (-np.arange(16, dtype=np.float32) / np.float32(16))
+    angle = (np.arange(GRID_W, dtype=np.float32)[:, None] * inverse[None, lane % 16]).astype(np.float64)
+    sign = np.where(lane % 32 < 16, -1.0, 1.0)[None, :]
+    return np.where(lane[None, :] < 64, np.cos(angle), sign * np.sin(angle)).astype(np.float32)
 
 
 def dot(a, b):
@@ -59,10 +38,19 @@
     return lax.dot_general(a, b, (((0,), (0,)), ((), ())), preferred_element_type=F32)
 
 
+def dot_nt(a, b):
+    return lax.dot_general(a, b, (((1,), (1,)), ((), ())), preferred_element_type=F32)
+
+
+def iota(shape, dim):
+    return lax.broadcasted_iota(jnp.int32, shape, dim)
+
+
 def kernel(
     nz, nx, cap,
-    q_ref, kv_ref, og_ref, pf_ref, pb_ref, pg_ref, wg_hbm, wu_hbm, wd_hbm, wo_hbm,
-    out_ref, fin_ref,
+    tab_ref, qg_ref, kg_ref, rt_ref, lg_ref, src_ref, pre_hbm, post_hbm, q_hbm, k_hbm, v_hbm, x_hbm, wg_hbm, wu_hbm, wd_hbm, wo_hbm,
+    out_ref, moe_ref,
+    qv, kv, vv, xv, prev, pg_ref, q_ref, kv_ref, og_ref, pb_ref,
     kvb, qb, qd, acc, ob, orx, wob, pa, ra,
     zrx, xsb, xb, wg, wu, wd, ga, up, tmp, own, pbuf, prx, psb, rs, ret, rbk, t2, fin,
     lsem, kxs, kxr, rrs, rrr, rls, rlr, qs, qr, ts, tr, wos, wor, as_, ar,
@@ -103,6 +91,15 @@
         copy.start()
         return copy
 
+    ep = z * nx + x
+    hl = pl.multiple_of((h // 2) * 128, 128)
+    mrow = pl.multiple_of(m * 128, 128)
+    lk = local(k_hbm.at[pl.ds(mrow, 128), pl.ds(hl, 128)], kv, 11)
+    lv = local(v_hbm.at[pl.ds(mrow, 128), pl.ds(hl, 128)], vv, 12)
+    lx = local(x_hbm, xv, 13)
+    lq = local(q_hbm, qv, 14)
+    lpre = local(pre_hbm, prev, 15)
+    lpost = local(post_hbm, pg_ref, 16)
     lwo = local(wo_hbm, wob.at[m], 0)
     lwg = local(wg_hbm, wg, 1)
     lwu = local(wu_hbm, wu, 2)
@@ -115,7 +112,71 @@
     peers += [(z, x, y, oc), (z, x, ysw, oc)]
     for peer in peers:
         pl.semaphore_signal(bar, inc=1, device_id=peer, device_id_type=MESH)
+
+    def mixer(j, l):
+        i = j - 64
+        return ((l < 64) & (i == l)) | ((l >= 64) & (i == ((l - 64) ^ 16)))
+
+    wide_mix = mixer(iota((192, 128), 0), iota((192, 128), 1)).astype(F32).astype(BF)
+    sub = lax.rem(h, 2)
+    hmix = mixer(iota((128, 128), 0) + (1 - sub) * 64, iota((128, 128), 1)).astype(F32).astype(BF)
+    qmix = wide_mix[64:128]
+    lane = iota((128, 128), 1)
+    row_lane = (lane & 63) < 32
+    col_table = tab_ref[...]
+
+    def gains(ref):
+        return jnp.dot(
+            jnp.broadcast_to(ref[...], (8, 64)), qmix.astype(F32), precision=lax.Precision.HIGHEST,
+            preferred_element_type=F32,
+        )[0:1]
+
+    def turned(values, gain, r):
+        table = jnp.where(row_lane, tab_ref[pl.ds(r, 1), :], col_table) * gain
+        scale = lax.rsqrt(jnp.mean(values * values, axis=1, keepdims=True) + EPSILON)
+        out = values * scale * table
+        return out + pltpu.roll(out, 64, 1)
+
+    kgain = gains(kg_ref)
+    lk.wait()
+    k128 = turned(dot(kv[...], hmix), kgain, ep * 4 + m)
+    kv_ref[0:64] = jnp.where(lane[0:64] < 64, k128[0:64], k128[64:128]).astype(BF)
+    lv.wait()
+    pick = (iota((64, 128), 1) == iota((64, 128), 0) + 64 * sub).astype(F32).astype(BF)
+    kv_ref[64:128] = dot_nt(pick, vv[...]).astype(BF)
     kvb[z, x] = kv_ref[...]
+
+    count = xv.shape[0]
+    experts = nz * nx
+    lx.wait()
+    x32 = xv[...].astype(F32)
+    xscale = lax.rsqrt(jnp.mean(x32 * x32, axis=1, keepdims=True) + EPSILON)
+    lpre.wait()
+    normed = []
+    for i in range(2):
+        col = pl.multiple_of((yy(4 * i) * 2 + c) * 128, 128)
+        normed.append((xv[:, pl.ds(col, 128)].astype(F32) * xscale * prev[:, pl.ds(col, 128)]).astype(BF))
+    normed = jnp.concatenate(normed, axis=1)
+    eid = iota((count, 128), 1)
+    eye = (iota((count, count), 1) == iota((count, count), 0)).astype(F32)
+    named = dot_nt(eye.astype(BF), rt_ref[...].astype(F32).astype(BF)).astype(jnp.int32)
+    hot = [eid == named[:, i : i + 1] for i in range(2)]
+    lower = (iota((count, count), 1) < iota((count, count), 0)).astype(F32).astype(BF)
+    rank = dot(lower, (hot[0] | hot[1]).astype(F32).astype(BF)) + (cap * eid).astype(F32)
+    place = [jnp.sum(jnp.where(hh, rank, 0.0), axis=1, keepdims=True).astype(jnp.int32) for hh in hot]
+    slot = iota((count, rows), 1)
+    pick = [slot == pp for pp in place]
+    og_ref[...] = dot_t((pick[0] | pick[1]).astype(F32).astype(BF), normed).astype(BF)
+    pb_ref[...] = (iota((rows, rows), 0) == src_ref[...]).astype(F32).astype(BF)
+
+    lq.wait()
+    q128 = dot_t(qv[...], qmix)
+    qgain = gains(qg_ref)
+    turned_q = [turned(q128[i * 128 : (i + 1) * 128], qgain, ep * 4 + i).astype(BF) for i in range(4)]
+    ordered = [turned_q[i][k * 32 : (k + 1) * 32] for k in range(4) for i in range(4)]
+    ordered = jnp.concatenate(ordered, axis=0) * BF(0.125)
+    pick_q = (iota((64, 128), 1) == iota((64, 128), 0)).astype(F32).astype(BF)
+    q_ref[...] = dot_nt(pick_q, ordered).astype(BF)
     qb[m] = q_ref[...]
     zrow = pl.multiple_of(z * zb, 16)
     zrx[pl.ds(zrow, zb), :] = og_ref[pl.ds(zrow, zb), :]
@@ -162,7 +223,7 @@
     for k in range(1, nz):
         frm = pl.multiple_of(zz(-k) * zb, 16)
         rc(og_ref.at[pl.ds(0, zb)], zrx.at[pl.ds(frm, zb)], zs.at[k], zr.at[k]).wait_recv()
-    xsb[...] = dot(pf_ref[...], zrx[...]).astype(BF)
+    xsb[...] = dot_t(pb_ref[...], zrx[...]).astype(BF)
     cl = pl.multiple_of(c * 128, 128)
     ocl = pl.multiple_of(oc * 128, 128)
     xrow = pl.multiple_of(x * xbk, 16)
@@ -355,12 +416,22 @@
         rc(pa.at[0], ra.at[k - 1], as_.at[k - 1], ar.at[k - 1]).wait_recv()
         mixed += ra[k - 1].astype(F32)
     scale = lax.rsqrt(jnp.mean(mixed * mixed, axis=1, keepdims=True) + EPSILON)
+    lpost.wait()
     out_ref[...] = (mixed * scale * pg_ref[...]).astype(BF)
+
+    logits = lg_ref[...]
+    grown = jnp.exp(logits - jnp.max(logits, axis=0, keepdims=True))
+    weight = lax.dot_general(
+        eye, grown / jnp.sum(grown, axis=0, keepdims=True), (((1,), (1,)), ((), ())),
+        precision=lax.Precision.HIGHEST, preferred_element_type=F32,
+    )
 
     for k in range(1, nz):
         frm = pl.multiple_of(zz(-k) * zb, 16)
         rc(t2.at[pl.ds(0, zb)], fin.at[pl.ds(frm, zb)], us.at[k], ur.at[k]).wait_recv()
-    fin_ref[...] = fin[...]
+    total = weight[:, 0:1] * dot(pick[0].astype(F32).astype(BF), fin[...])
+    total += weight[:, 1:2] * dot(pick[1].astype(F32).astype(BF), fin[...])
+    moe_ref[...] = total.astype(BF)
     for copy in sent:
         copy.wait_send()
 
@@ -368,30 +439,32 @@
 def call(nz, nx, cap, *args):
     rows = nz * nx * cap
     vm = pl.BlockSpec(memory_space=pltpu.VMEM)
-    hbm = pl.BlockSpec(memory_space=pl.ANY)
+    hbm = pl.BlockSpec(memory_space=pltpu.HBM)
     dma = lambda *n: pltpu.SemaphoreType.DMA(n)
     big = lambda *s: pltpu.VMEM(s, BF)
     wide = lambda *s: pltpu.VMEM(s, F32)
     scratch = [
+        big(64, 512), big(128, 128), big(128, 128), big(128, 2048), wide(1, 2048), wide(1, 2048),
+        big(64, 512), big(128, 128), big(rows, 256), big(rows, rows),
         big(nz, nx, 128, 128), big(4, 64, 512), big(8, 128, 512), wide(8, ODIM, 256), big(8, ODIM, 256),
         big(3, 2, ODIM, 256), big(4, 64, 2048), big(4, 32, 2048), big(3, 32, 2048),
         big(rows, 256), big(rows, 256), big(NY, rows, 256), big(2048, 256), big(2048, 256), big(NY, 256, 256),
         wide(rows, 256), wide(rows, 256), wide(2, rows, 256), wide(NY, rows, 128), big(NY, rows, 128),
         big(NY, rows, 128), big(NY, rows, 128), big(7, rows, 128), big(rows, 128), big(rows, 128),
         big(rows, 128), big(rows, 128),
-        dma(11), dma(nx), dma(nx), dma(nz), dma(nz), dma(nz), dma(nz), dma(3), dma(3), dma(3), dma(3), dma(3), dma(3),
+        dma(17), dma(nx), dma(nx), dma(nz), dma(nz), dma(nz), dma(nz), dma(3), dma(3), dma(3), dma(3), dma(3), dma(3),
         dma(3), dma(3),
         dma(nz), dma(nz), dma(2, nx), dma(2, nx), dma(6), dma(6), dma(8), dma(8), dma(8), dma(8), dma(7), dma(7),
         dma(nx), dma(nx), dma(nz), dma(nz),
     ]
     return pl.pallas_call(
         functools.partial(kernel, nz, nx, cap),
-        out_shape=(jax.ShapeDtypeStruct((32, 2048), BF), jax.ShapeDtypeStruct((rows, 128), BF)),
-        in_specs=[vm] * 6 + [hbm] * 4,
+        out_shape=(jax.ShapeDtypeStruct((32, 2048), BF), jax.ShapeDtypeStruct((128, 128), BF)),
+        in_specs=[vm] * 6 + [hbm] * 10,
         out_specs=(vm, vm),
         scratch_shapes=scratch,
         compiler_params=pltpu.CompilerParams(
-            collective_id=0, has_side_effects=True, vmem_limit_bytes=48 * 1024 * 1024
+            collective_id=0, has_side_effects=True, vmem_limit_bytes=67043328
         ),
         name="layer",
     )(*args)
@@ -401,51 +474,16 @@
     q_in, k_in, v_in, q_gain, k_gain, w_out, post_gain, moe_in, routes, route_logits, pre_gain, w_gate, w_up, w_down
 ):
     nz, nx = lax.axis_size("z"), lax.axis_size("x")
-    y, c = lax.axis_index("y"), lax.axis_index("c")
-    ep = lax.axis_index(EP)
     count, top = routes.shape
     experts = nz * nx
     cap = max(2, 3 * top * count // (2 * experts))
-    rows = experts * cap
-    offset = ep * 512
-    h = y // 2
-    m = lax.rem(y, 2) * 2 + c
-
-    q = grid_rotary(head_norm(q_in.astype(F32), q_gain), offset).astype(BF) * BF(0.125)
-    q = jnp.transpose(q.reshape(4, 4, 32, 64), (3, 1, 0, 2)).reshape(64, 512)
-    k = lax.dynamic_slice(k_in, (m * 128, h * 64), (128, 64)).astype(F32)
-    k = grid_rotary(head_norm(k, k_gain), offset + m * 128).astype(BF)
-    v = lax.dynamic_slice(v_in, (m * 128, h * 64), (128, 64))
-    kv = jnp.concatenate([jnp.concatenate([k[:64], k[64:]], axis=1), v.T], axis=0)
-
-    x32 = moe_in.astype(F32)
-    scale = lax.rsqrt(jnp.mean(x32 * x32, axis=-1, keepdims=True) + EPSILON)
-    cols = [(lax.rem(y + 4 * i, NY) * 2 + c) * 128 for i in range(2)]
-    xs = [lax.dynamic_slice(moe_in, (0, col), (count, 128)).astype(F32) for col in cols]
-    gs = [lax.dynamic_slice(pre_gain, (col,), (128,)) for col in cols]
-    xn = jnp.concatenate([(v_ * scale * g_).astype(BF) for v_, g_ in zip(xs, gs)], axis=1)
-    rt = routes.T
-    eid = jnp.arange(experts, dtype=jnp.int32)[:, None]
-    hot = [(eid == rt[i][None, :]) for i in range(top)]
-    both = (hot[0] | hot[1]).astype(BF)
-    tri = (jnp.arange(count)[:, None] < jnp.arange(count)[None, :]).astype(BF)
-    rank = dot(both, tri).astype(jnp.int32)
-    place = [jnp.sum(jnp.where(hh, rank + cap * eid, 0), axis=0) for hh in hot]
-    slot = jnp.arange(rows, dtype=jnp.int32)[:, None]
-    sel = [(slot == pp[None, :]) for pp in place]
-    og = dot((sel[0] | sel[1]).astype(BF), xn).astype(BF)
-
-    i = jnp.arange(rows, dtype=jnp.int32)
+    i = np.arange(experts * cap, dtype=np.int32)
     src = (i % (nz * cap)) // cap * (nx * cap) + i // (nz * cap) * cap + i % cap
-    pf = (src[:, None] == i[None, :]).astype(BF)
-    pb = (src[None, :] == i[:, None]).astype(BF)
-
-    attn, fin = call(
-        nz, nx, cap, q, kv, og, pf, pb, post_gain[None, :], w_gate[0], w_up[0], w_down[0], w_out
+    return call(
+        nz, nx, cap, jnp.asarray(angle_table()), q_gain[None, :], k_gain[None, :], routes.T, route_logits.T,
+        jnp.asarray(src[None, :]), pre_gain[None, :], post_gain[None, :],
+        q_in.T, k_in, v_in, moe_in, w_gate[0], w_up[0], w_down[0], w_out,
     )
-    weight = jax.nn.softmax(route_logits, axis=-1)
-    moe = sum(weight[:, j : j + 1] * dot_t(sel[j].astype(BF), fin) for j in range(top))
-    return attn, moe.astype(BF)
 
 
 def solution(mesh):

time: 103 us -> 84 us (0.82)
  local copies, waits for them, and re-layouts: 12.5 us -> 2.19 us
  other arithmetic: 8.02 us -> 0 us
  matrix products: 1.48 us -> 0 us
  Pallas kernels: 79.6 us -> 80.9 us
    concatenate x8 -> x0, local copies, waits for them, and re-layouts: 5.82 us -> none  [grid_rotary(): jnp.concatenate([rotate_half(values[:, :half], grid_row[:, None] * invers...]
    mul x4 -> x0, other arithmetic: 2.8 us -> none  [the longest x1 1.87 us: per_device(): grid_rotary(head_norm(q_in.astype(F32), q_gain), offset).astype(BF)]
    unnamed x26 -> x4, local copies, waits for them, and re-layouts: 4.78 us -> 2.19 us
    reduce_sum x4 -> x0, other arithmetic: 2.22 us -> none  [the longest x1 1.23 us: per_device(): scale = lax.rsqrt(jnp.mean(x32 * x32, axis=-1, keepdims=True) + EPSILON)]
    dot_general x4 -> x0, matrix products: 1.48 us -> none  [the longest x2 1.13 us: dot_t(): lax.dot_general(a, b, (((0,), (0,)), ((), ())), preferred_element_type=F32)]
    pallas_call x1, Pallas kernels: 79.6 us -> 80.9 us  [call(): pl.pallas_call(functools.partial(kernel, nz, nx, cap), out_shape=(jax.Sha...]
    convert_element_type x4 -> x0, other arithmetic: 1.06 us -> none  [the longest x1 0.86 us: per_device(): (v_ * scale * g_).astype(BF)]
where the time goes in v2:
time: 84 us; the launch traced here: 83.8 us
  Pallas kernels  80.9 us (96%)
  local copies, waits for them, and re-layouts  2.19 us (3%)
    pallas_call x1, Pallas kernels, call(): pl.pallas_call(functools.partial(kernel, nz, nx, cap), out_shape=(jax.Sha...  80.9 us
    unnamed x4, local copies, waits for them, and re-layouts  2.19 us

profile of v2, /device:TPU:1, one launch (start us, length us, event | category | flops | bytes accessed | tf_op | source)
XLA Modules:
  0.0 83.8 jit_solution(8958426936648955390)
XLA Ops:
  0.6 80.9 %layer.1 = (bf16[32,2048]{1,0:T(8,128)(2,1)}, bf16[128,128]{1,0:T(8,128)(2,1)}) custom-call(f32[128,128]{1,0:T(8,128)} %constant.4.clone.tab_ref, f32[1,64]{1,0:T(1,128)} %bitcast.18, f32[1,64]{1,0:T(1,128)} %bitcast.19, s32[2,128]{1,0:T(2,128)} %bitcast.16, f32[2,128]{1,0:T(2,128)} %bitcast.17, s32[1,384]{1,0:T(1,128)} %constant.5.clone.src_ref, ...), custom_call_target="tpu_custom_call" | custom-call | tf_op jit(solution)/shard_map/layer/pallas_call | solution.py:460
  81.6 0.0 copy-start
  81.6 1.6 %copy.20 = bf16[32,2048]{1,0:T(8,128)(2,1)} copy(bf16[32,2048]{1,0:T(8,128)(2,1)} %get-tuple-element.4) | data formatting | bytes 262144
  83.2 0.0 copy-done
  83.2 0.6 copy.21
Async XLA Ops:
  81.6 1.6 %copy-start = (bf16[128,128]{1,0:T(8,128)(2,1)S(1)}, bf16[128,128]{1,0:T(8,128)(2,1)}, u32[]{:S(2)}) copy-start(bf16[128,128]{1,0:T(8,128)(2,1)} %get-tuple-element.5) | copy-start | bytes 98308

commit v3 on v2

--- a/solution.py
+++ b/solution.py
@@ -182,11 +182,11 @@
     zrx[pl.ds(zrow, zb), :] = og_ref[pl.ds(zrow, zb), :]
     pl.semaphore_wait(bar, len(peers))
 
-    for k in range(1, nx):
-        send(kv_ref, kvb.at[z, x], kxs.at[k], kxr.at[k], dx=xx(k))
     for k in range(1, nz):
         to = pl.multiple_of(zz(k) * zb, 16)
         send(og_ref.at[pl.ds(to, zb)], zrx.at[pl.ds(zrow, zb)], zs.at[k], zr.at[k], dz=zz(k))
+    for k in range(1, nx):
+        send(kv_ref, kvb.at[z, x], kxs.at[k], kxr.at[k], dx=xx(k))
     send(q_ref, qb.at[m], qs.at[0], qr.at[0], dc=oc)
     send(q_ref, qb.at[m], qs.at[1], qr.at[1], dy=ysw)
     send(q_ref, qb.at[m], qs.at[2], qr.at[2], dy=ysw, dc=oc)
@@ -195,30 +195,34 @@
         qd[j] = jnp.zeros((128, 512), BF)
         acc[j] = jnp.zeros((ODIM, 256), F32)
 
-    for k in range(1, nx):
-        rc(kv_ref, kvb.at[z, xx(-k)], kxs.at[k], kxr.at[k]).wait_recv()
-
-    def ring(step):
+    def ring(step, i):
         if step < nz // 2:
-            g = kvb.at[zz(-step)]
-            send(g, g, rrs.at[step], rrr.at[step], dz=zz(1))
+            g = kvb.at[zz(-step), xx(i)]
+            send(g, g, rrs.at[step, i], rrr.at[step, i], dz=zz(1))
         if step < (nz - 1) // 2:
-            g = kvb.at[zz(step)]
-            send(g, g, rls.at[step], rlr.at[step], dz=zz(-1))
+            g = kvb.at[zz(step), xx(i)]
+            send(g, g, rls.at[step, i], rlr.at[step, i], dz=zz(-1))
 
     def ring_wait(step):
         got = []
         if step < nz // 2:
-            g = kvb.at[zz(-step - 1)]
-            rc(g, g, rrs.at[step], rrr.at[step]).wait_recv()
             got.append(zz(-step - 1))
         if step < (nz - 1) // 2:
-            g = kvb.at[zz(step + 1)]
-            rc(g, g, rls.at[step], rlr.at[step]).wait_recv()
             got.append(zz(step + 1))
+        for i in range(nx):
+            if step < nz // 2:
+                g = kvb.at[zz(-step - 1), xx(i)]
+                rc(g, g, rrs.at[step, i], rrr.at[step, i]).wait_recv()
+            if step < (nz - 1) // 2:
+                g = kvb.at[zz(step + 1), xx(i)]
+                rc(g, g, rls.at[step, i], rlr.at[step, i]).wait_recv()
+            ring(step + 1, i)
         return got
 
-    ring(0)
+    ring(0, 0)
+    for k in range(1, nx):
+        rc(kv_ref, kvb.at[z, xx(-k)], kxs.at[k], kxr.at[k]).wait_recv()
+        ring(0, nx - k)
 
     for k in range(1, nz):
         frm = pl.multiple_of(zz(-k) * zb, 16)
@@ -255,16 +259,23 @@
         vals = jnp.concatenate(vals, axis=1)
         vals = jnp.concatenate([vals, jnp.ones((ODIM - 64, nx * 128), BF)], axis=0)
 
-        def tile(j, carry):
-            p = jnp.exp(dot(keys, qd[j])).astype(BF)
+        def project(p):
             parts = []
             for i in range(nx):
                 parts.append(p[i * 64 : (i + 1) * 64, 0:256])
                 parts.append(p[i * 64 : (i + 1) * 64, 256:512])
-            acc[j] += dot(vals, jnp.concatenate(parts, axis=0))
-            return carry
-
-        lax.fori_loop(0, 8, tile, 0)
+            return jnp.concatenate(parts, axis=0)
+
+        scores = [dot(keys, qd[0]), dot(keys, qd[1])]
+        held = None
+        for j in range(8):
+            p = project(jnp.exp(scores[j]).astype(BF))
+            if j < 6:
+                scores.append(dot(keys, qd[j + 2]))
+            if held is not None:
+                acc[j - 1] += dot(vals, held)
+            held = p
+        acc[7] += dot(vals, held)
 
     attend(z)
 
@@ -302,34 +313,12 @@
         swap((r - k + NY) % NY)
 
     steps = max(nz // 2, (nz - 1) // 2)
-    for step in range(steps):
-        got = ring_wait(step)
-        ring(step + 1)
-        if step == steps - 2:
-            for i in range(4):
-                arrive(i)
-        for zi in got:
+    for step in range(max(steps - 2, 0)):
+        for zi in ring_wait(step):
             attend(zi)
-    if steps < 2:
-        for i in range(4):
-            arrive(i)
-    for i in range(4, 6):
+    for i in range(6):
         arrive(i)
-
-    for j in range(8):
-        a = acc[j]
-        den = a[64:ODIM]
-        hi = den.astype(BF)
-        lo = (den - hi.astype(F32)).astype(BF)
-        first = lax.broadcasted_iota(jnp.int32, (ODIM - 64, 256), 0) == 0
-        ob[j, 0:64] = a[0:64].astype(BF)
-        ob[j, 64:ODIM] = jnp.where(first, hi.astype(F32), lo.astype(F32)).astype(BF)
-    other = wob.at[(1 - b) * 2 + c]
-    rc(other, other, wos.at[1], wor.at[1]).wait_recv()
-    send(other, other, wos.at[2], wor.at[2], dc=oc)
-    members = ((0, y, oc, b * 2 + oc), (1, ysw, c, (1 - b) * 2 + c), (2, ysw, oc, (1 - b) * 2 + oc))
-    for i, dy, dc, mm in members:
-        send(ob.at[pl.ds(2 * mm, 2)], orx.at[i], ts.at[i], tr.at[i], dy=dy, dc=dc)
+    later = ring_wait(steps - 2) if steps > 1 else []
 
     lwg.wait()
     lwu.wait()
@@ -369,6 +358,37 @@
         rc(psb.at[0], rs.at[i], ms.at[i], mr.at[i]).wait_recv()
         return rs[i].astype(F32)
 
+    other = wob.at[(1 - b) * 2 + c]
+    rc(other, other, wos.at[1], wor.at[1]).wait_recv()
+    send(other, other, wos.at[2], wor.at[2], dc=oc)
+    for zi in later:
+        attend(zi)
+    far_sum = got_rs(0)
+    right = c.astype(F32)
+    psb[2] = (paired(2) + got_rs(1) + far_sum * right).astype(BF)
+    send(psb.at[2], rs.at[5], ms.at[5], mr.at[5], dy=yy(2))
+    psb[6] = (paired(6) + got_rs(2) + far_sum * (1.0 - right)).astype(BF)
+    send(psb.at[6], rs.at[6], ms.at[6], mr.at[6], dy=yy(-2))
+
+    for zi in ring_wait(steps - 1):
+        attend(zi)
+    for j in range(8):
+        a = acc[j]
+        den = a[64:ODIM]
+        hi = den.astype(BF)
+        lo = (den - hi.astype(F32)).astype(BF)
+        first = lax.broadcasted_iota(jnp.int32, (ODIM - 64, 256), 0) == 0
+        ob[j, 0:64] = a[0:64].astype(BF)
+        ob[j, 64:ODIM] = jnp.where(first, hi.astype(F32), lo.astype(F32)).astype(BF)
+    members = ((0, y, oc, b * 2 + oc), (1, ysw, c, (1 - b) * 2 + c), (2, ysw, oc, (1 - b) * 2 + oc))
+    for i, dy, dc, mm in members:
+        send(ob.at[pl.ds(2 * mm, 2)], orx.at[i], ts.at[i], tr.at[i], dy=dy, dc=dc)
+
+    ret[...] = (paired(0) + got_rs(3) + got_rs(4) + got_rs(5) + got_rs(6)).astype(BF)
+    rbk[pl.ds(xrow, xbk), :] = ret[pl.ds(xrow, xbk), :]
+    for k in range(1, nx):
+        to = pl.multiple_of(xx(k) * xbk, 16)
+        send(ret.at[pl.ds(to, xbk)], rbk.at[pl.ds(xrow, xbk)], vs.at[k], vr.at[k], dx=xx(k))
     for i, dy, dc, mm in members:
         rc(ob.at[pl.ds(0, 2)], orx.at[i], ts.at[i], tr.at[i]).wait_recv()
     heads = []
@@ -387,21 +407,9 @@
         part = dot_t(hot, wob[:, :, n * 512 : (n + 1) * 512].reshape(256, 512))
         pa[:, :, n * 512 : (n + 1) * 512] = part.astype(BF).reshape(4, 32, 512)
 
-    far_sum = got_rs(0)
-    right = c.astype(F32)
-    psb[2] = (paired(2) + got_rs(1) + far_sum * right).astype(BF)
-    send(psb.at[2], rs.at[5], ms.at[5], mr.at[5], dy=yy(2))
-    psb[6] = (paired(6) + got_rs(2) + far_sum * (1.0 - right)).astype(BF)
-    send(psb.at[6], rs.at[6], ms.at[6], mr.at[6], dy=yy(-2))
-
     for k in range(1, 4):
         send(pa.at[lax.rem(h + k, 4)], ra.at[k - 1], as_.at[k - 1], ar.at[k - 1], dy=yy(2 * k))
 
-    ret[...] = (paired(0) + got_rs(3) + got_rs(4) + got_rs(5) + got_rs(6)).astype(BF)
-    rbk[pl.ds(xrow, xbk), :] = ret[pl.ds(xrow, xbk), :]
-    for k in range(1, nx):
-        to = pl.multiple_of(xx(k) * xbk, 16)
-        send(ret.at[pl.ds(to, xbk)], rbk.at[pl.ds(xrow, xbk)], vs.at[k], vr.at[k], dx=xx(k))
     for k in range(1, nx):
         frm = pl.multiple_of(xx(-k) * xbk, 16)
         rc(ret.at[pl.ds(0, xbk)], rbk.at[pl.ds(frm, xbk)], vs.at[k], vr.at[k]).wait_recv()
@@ -452,7 +460,7 @@
         wide(rows, 256), wide(rows, 256), wide(2, rows, 256), wide(NY, rows, 128), big(NY, rows, 128),
         big(NY, rows, 128), big(NY, rows, 128), big(7, rows, 128), big(rows, 128), big(rows, 128),
         big(rows, 128), big(rows, 128),
-        dma(17), dma(nx), dma(nx), dma(nz), dma(nz), dma(nz), dma(nz), dma(3), dma(3), dma(3), dma(3), dma(3), dma(3),
+        dma(17), dma(nx), dma(nx), dma(nz, nx), dma(nz, nx), dma(nz, nx), dma(nz, nx), dma(3), dma(3), dma(3), dma(3), dma(3), dma(3),
         dma(3), dma(3),
         dma(nz), dma(nz), dma(2, nx), dma(2, nx), dma(6), dma(6), dma(8), dma(8), dma(8), dma(8), dma(7), dma(7),
         dma(nx), dma(nx), dma(nz), dma(nz),
@@ -464,7 +472,7 @@
         out_specs=(vm, vm),
         scratch_shapes=scratch,
         compiler_params=pltpu.CompilerParams(
-            collective_id=0, has_side_effects=True, vmem_limit_bytes=67043328
+            collective_id=0, has_side_effects=True, vmem_limit_bytes=67043328 - 200 * 1024
         ),
         name="layer",
     )(*args)

time: 84 us -> 80.3 us (0.956)
  Pallas kernels: 80.9 us -> 77.1 us
    pallas_call x1, Pallas kernels: 80.9 us -> 77.1 us  [call(): pl.pallas_call(functools.partial(kernel, nz, nx, cap), out_shape=(jax.Sha...]
where the time goes in v3:
time: 80.3 us; the launch traced here: 80 us
  Pallas kernels  77.1 us (96%)
  local copies, waits for them, and re-layouts  2.19 us (3%)
    pallas_call x1, Pallas kernels, call(): pl.pallas_call(functools.partial(kernel, nz, nx, cap), out_shape=(jax.Sha...  77.1 us
    unnamed x4, local copies, waits for them, and re-layouts  2.19 us

profile of v3, /device:TPU:1, one launch (start us, length us, event | category | flops | bytes accessed | tf_op | source)
XLA Modules:
  0.0 80.0 jit_solution(16734705659280100154)
XLA Ops:
  0.6 77.1 %layer.1 = (bf16[32,2048]{1,0:T(8,128)(2,1)}, bf16[128,128]{1,0:T(8,128)(2,1)}) custom-call(f32[128,128]{1,0:T(8,128)} %constant.4.clone.tab_ref, f32[1,64]{1,0:T(1,128)} %bitcast.18, f32[1,64]{1,0:T(1,128)} %bitcast.19, s32[2,128]{1,0:T(2,128)} %bitcast.16, f32[2,128]{1,0:T(2,128)} %bitcast.17, s32[1,384]{1,0:T(1,128)} %constant.5.clone.src_ref, ...), custom_call_target="tpu_custom_call" | custom-call | tf_op jit(solution)/shard_map/layer/pallas_call | solution.py:468
  77.8 0.0 copy-start
  77.8 1.6 %copy.20 = bf16[32,2048]{1,0:T(8,128)(2,1)} copy(bf16[32,2048]{1,0:T(8,128)(2,1)} %get-tuple-element.4) | data formatting | bytes 262144
  79.3 0.0 copy-done
  79.3 0.6 copy.21
Async XLA Ops:
  77.8 1.6 %copy-start = (bf16[128,128]{1,0:T(8,128)(2,1)S(1)}, bf16[128,128]{1,0:T(8,128)(2,1)}, u32[]{:S(2)}) copy-start(bf16[128,128]{1,0:T(8,128)(2,1)} %get-tuple-element.5) | copy-start | bytes 98308

commit v4 on v3

--- a/solution.py
+++ b/solution.py
@@ -51,9 +51,9 @@
     tab_ref, qg_ref, kg_ref, rt_ref, lg_ref, src_ref, pre_hbm, post_hbm, q_hbm, k_hbm, v_hbm, x_hbm, wg_hbm, wu_hbm, wd_hbm, wo_hbm,
     out_ref, moe_ref,
     qv, kv, vv, xv, prev, pg_ref, q_ref, kv_ref, og_ref, pb_ref,
-    kvb, qb, qd, acc, ob, orx, wob, pa, ra,
+    kvb, qb, qd, acc, ob, orx, wall, ho, hb,
     zrx, xsb, xb, wg, wu, wd, ga, up, tmp, own, pbuf, prx, psb, rs, ret, rbk, t2, fin,
-    lsem, kxs, kxr, rrs, rrr, rls, rlr, qs, qr, ts, tr, wos, wor, as_, ar,
+    lsem, kxs, kxr, rrs, rrr, rls, rlr, qs, qr, ts, tr, wys, wyr, wxs, wxr, wds, wdr, as_, ar,
     zs, zr, xs, xr, ys, yr, ds, dr, es, er, ms, mr, vs, vr, us, ur,
 ):
     z, x, y, c = (lax.axis_index(n) for n in ALL)
@@ -100,7 +100,8 @@
     lq = local(q_hbm, qv, 14)
     lpre = local(pre_hbm, prev, 15)
     lpost = local(post_hbm, pg_ref, 16)
-    lwo = local(wo_hbm, wob.at[m], 0)
+    wc = 2048 // nx
+    lwo = local(wo_hbm.at[:, pl.ds(pl.multiple_of(x * wc, 128), wc)], wall.at[x, c, y], 0)
     lwg = local(wg_hbm, wg, 1)
     lwu = local(wu_hbm, wu, 2)
     lwd = [local(wd_hbm.at[:, k * 256 : (k + 1) * 256], wd.at[k], 3 + k) for k in range(NY)]
@@ -108,7 +109,7 @@
     bar = pltpu.get_barrier_semaphore()
     peers = [(zz(k), x, y, c) for k in range(1, nz)]
     peers += [(z, xx(k), y, c) for k in range(1, nx)]
-    peers += [(z, x, yy(k), c) for k in (1, -1, 2, -2, 4)]
+    peers += [(z, x, yy(k), c) for k in (1, -1, 2, -2, 3, -3, 4)]
     peers += [(z, x, y, oc), (z, x, ysw, oc)]
     for peer in peers:
         pl.semaphore_signal(bar, inc=1, device_id=peer, device_id_type=MESH)
@@ -191,6 +192,10 @@
     send(q_ref, qb.at[m], qs.at[1], qr.at[1], dy=ysw)
     send(q_ref, qb.at[m], qs.at[2], qr.at[2], dy=ysw, dc=oc)
 
+    lwo.wait()
+    for k in (1, 7, 2, 6, 3, 5, 4):
+        send(wall.at[x, c, y], wall.at[x, c, y], wys.at[k], wyr.at[k], dy=yy(k))
+
     for j in range(8):
         qd[j] = jnp.zeros((128, 512), BF)
         acc[j] = jnp.zeros((ODIM, 256), F32)
@@ -302,9 +307,12 @@
 
     swap(0)
     swap(4)
-    lwo.wait()
-    send(wob.at[m], wob.at[m], wos.at[0], wor.at[0], dc=oc)
-    send(wob.at[m], wob.at[m], wos.at[1], wor.at[1], dy=ysw)
+    for k in range(1, NY):
+        g = wall.at[x, c, yy(-k)]
+        rc(g, g, wys.at[k], wyr.at[k]).wait_recv()
+    for k in range(1, nx):
+        send(wall.at[x, c], wall.at[x, c], wxs.at[k], wxr.at[k], dx=xx(k))
+    send(wall.at[x, c], wall.at[x, c], wds.at[0], wdr.at[0], dc=oc)
 
     def arrive(i):
         k, r = plan[i]
@@ -358,11 +366,12 @@
         rc(psb.at[0], rs.at[i], ms.at[i], mr.at[i]).wait_recv()
         return rs[i].astype(F32)
 
-    other = wob.at[(1 - b) * 2 + c]
-    rc(other, other, wos.at[1], wor.at[1]).wait_recv()
-    send(other, other, wos.at[2], wor.at[2], dc=oc)
     for zi in later:
         attend(zi)
+    for k in range(1, nx):
+        g = wall.at[xx(-k), c]
+        rc(g, g, wxs.at[k], wxr.at[k]).wait_recv()
+        send(g, g, wds.at[k], wdr.at[k], dc=oc)
     far_sum = got_rs(0)
     right = c.astype(F32)
     psb[2] = (paired(2) + got_rs(1) + far_sum * right).astype(BF)
@@ -398,17 +407,12 @@
             t += orx[i, rp].astype(F32)
         o = (t[0:64] / (t[64:65] + t[65:66])).astype(BF)
         heads += [o[:, 0:128], o[:, 128:256]]
-    hot = jnp.concatenate(heads, axis=0)
-    partner = wob.at[b * 2 + oc]
-    rc(partner, partner, wos.at[0], wor.at[0]).wait_recv()
-    far = wob.at[(1 - b) * 2 + oc]
-    rc(far, far, wos.at[2], wor.at[2]).wait_recv()
-    for n in range(4):
-        part = dot_t(hot, wob[:, :, n * 512 : (n + 1) * 512].reshape(256, 512))
-        pa[:, :, n * 512 : (n + 1) * 512] = part.astype(BF).reshape(4, 32, 512)
-
+    heads = jnp.concatenate(heads, axis=0)
+    square = (iota((256, 256), 0) == iota((256, 256), 1)).astype(F32).astype(BF)
+    ho[...] = dot_t(heads, square).astype(BF).reshape(4, 32, 256)
+    hb[h] = ho[h]
     for k in range(1, 4):
-        send(pa.at[lax.rem(h + k, 4)], ra.at[k - 1], as_.at[k - 1], ar.at[k - 1], dy=yy(2 * k))
+        send(ho.at[lax.rem(h + k, 4)], hb.at[h], as_.at[k - 1], ar.at[k - 1], dy=yy(2 * k))
 
     for k in range(1, nx):
         frm = pl.multiple_of(xx(-k) * xbk, 16)
@@ -419,10 +423,20 @@
         to = pl.multiple_of(zz(k) * zb, 16)
         send(t2.at[pl.ds(to, zb)], fin.at[pl.ds(zrow, zb)], us.at[k], ur.at[k], dz=zz(k))
 
-    mixed = pa[h].astype(F32)
+    for k in range(1, nx):
+        g = wall.at[xx(-k), oc]
+        rc(g, g, wds.at[k], wdr.at[k]).wait_recv()
+    rc(wall.at[x, oc], wall.at[x, oc], wds.at[0], wdr.at[0]).wait_recv()
     for k in range(1, 4):
-        rc(pa.at[0], ra.at[k - 1], as_.at[k - 1], ar.at[k - 1]).wait_recv()
-        mixed += ra[k - 1].astype(F32)
+        rc(ho.at[0], hb.at[lax.rem(h - k + 4, 4)], as_.at[k - 1], ar.at[k - 1]).wait_recv()
+    columns = []
+    for n in range(nx):
+        part = None
+        for g in range(4):
+            w = jnp.concatenate([wall[n, r % 2, 2 * g + r // 2] for r in range(4)], axis=0)
+            part = dot(hb[g], w) if part is None else part + dot(hb[g], w)
+        columns.append(part)
+    mixed = jnp.concatenate(columns, axis=1)
     scale = lax.rsqrt(jnp.mean(mixed * mixed, axis=1, keepdims=True) + EPSILON)
     lpost.wait()
     out_ref[...] = (mixed * scale * pg_ref[...]).astype(BF)
@@ -455,13 +469,13 @@
         big(64, 512), big(128, 128), big(128, 128), big(128, 2048), wide(1, 2048), wide(1, 2048),
         big(64, 512), big(128, 128), big(rows, 256), big(rows, rows),
         big(nz, nx, 128, 128), big(4, 64, 512), big(8, 128, 512), wide(8, ODIM, 256), big(8, ODIM, 256),
-        big(3, 2, ODIM, 256), big(4, 64, 2048), big(4, 32, 2048), big(3, 32, 2048),
+        big(3, 2, ODIM, 256), big(nx, 2, NY, 64, 2048 // nx), big(4, 32, 256), big(4, 32, 256),
         big(rows, 256), big(rows, 256), big(NY, rows, 256), big(2048, 256), big(2048, 256), big(NY, 256, 256),
         wide(rows, 256), wide(rows, 256), wide(2, rows, 256), wide(NY, rows, 128), big(NY, rows, 128),
         big(NY, rows, 128), big(NY, rows, 128), big(7, rows, 128), big(rows, 128), big(rows, 128),
         big(rows, 128), big(rows, 128),
-        dma(17), dma(nx), dma(nx), dma(nz, nx), dma(nz, nx), dma(nz, nx), dma(nz, nx), dma(3), dma(3), dma(3), dma(3), dma(3), dma(3),
-        dma(3), dma(3),
+        dma(17), dma(nx), dma(nx), dma(nz, nx), dma(nz, nx), dma(nz, nx), dma(nz, nx), dma(3), dma(3), dma(3), dma(3), dma(NY), dma(NY), dma(nx), dma(nx),
+        dma(nx), dma(nx), dma(3), dma(3),
         dma(nz), dma(nz), dma(2, nx), dma(2, nx), dma(6), dma(6), dma(8), dma(8), dma(8), dma(8), dma(7), dma(7),
         dma(nx), dma(nx), dma(nz), dma(nz),
     ]

time: 80.3 us -> 76.6 us (0.954)
  the two profiles are of different devices: /device:TPU:1 before, /device:TPU:16 now
where the time goes in v4:
time: 76.6 us; the launch traced here: 76.4 us
  Pallas kernels  73.6 us (96%)
  local copies, waits for them, and re-layouts  2.19 us (3%)
    pallas_call x1, Pallas kernels, call(): pl.pallas_call(functools.partial(kernel, nz, nx, cap), out_shape=(jax.Sha...  73.6 us
    unnamed x4, local copies, waits for them, and re-layouts  2.19 us

profile of v4, /device:TPU:16, one launch (start us, length us, event | category | flops | bytes accessed | tf_op | source)
XLA Modules:
  0.0 76.4 jit_solution(9714454739771491721)
XLA Ops:
  0.6 73.6 %layer.1 = (bf16[32,2048]{1,0:T(8,128)(2,1)}, bf16[128,128]{1,0:T(8,128)(2,1)}) custom-call(f32[128,128]{1,0:T(8,128)} %constant.4.clone.tab_ref, f32[1,64]{1,0:T(1,128)} %bitcast.18, f32[1,64]{1,0:T(1,128)} %bitcast.19, s32[2,128]{1,0:T(2,128)} %bitcast.16, f32[2,128]{1,0:T(2,128)} %bitcast.17, s32[1,384]{1,0:T(1,128)} %constant.5.clone.src_ref, ...), custom_call_target="tpu_custom_call" | custom-call | tf_op jit(solution)/shard_map/layer/pallas_call | solution.py:482
  74.2 0.0 copy-start
  74.3 1.6 %copy.20 = bf16[32,2048]{1,0:T(8,128)(2,1)} copy(bf16[32,2048]{1,0:T(8,128)(2,1)} %get-tuple-element.4) | data formatting | bytes 262144
  75.8 0.0 copy-done
  75.8 0.6 copy.21
Async XLA Ops:
  74.2 1.6 %copy-start = (bf16[128,128]{1,0:T(8,128)(2,1)S(1)}, bf16[128,128]{1,0:T(8,128)(2,1)}, u32[]{:S(2)}) copy-start(bf16[128,128]{1,0:T(8,128)(2,1)} %get-tuple-element.5) | copy-start | bytes 98308

commit v5 on v4

--- a/solution.py
+++ b/solution.py
@@ -183,7 +183,7 @@
     zrx[pl.ds(zrow, zb), :] = og_ref[pl.ds(zrow, zb), :]
     pl.semaphore_wait(bar, len(peers))
 
-    for k in range(1, nz):
+    for k in sorted(range(1, nz), key=lambda d: -min(d, nz - d)):
         to = pl.multiple_of(zz(k) * zb, 16)
         send(og_ref.at[pl.ds(to, zb)], zrx.at[pl.ds(zrow, zb)], zs.at[k], zr.at[k], dz=zz(k))
     for k in range(1, nx):
@@ -224,11 +224,6 @@
             ring(step + 1, i)
         return got
 
-    ring(0, 0)
-    for k in range(1, nx):
-        rc(kv_ref, kvb.at[z, xx(-k)], kxs.at[k], kxr.at[k]).wait_recv()
-        ring(0, nx - k)
-
     for k in range(1, nz):
         frm = pl.multiple_of(zz(-k) * zb, 16)
         rc(og_ref.at[pl.ds(0, zb)], zrx.at[pl.ds(frm, zb)], zs.at[k], zr.at[k]).wait_recv()
@@ -239,7 +234,7 @@
     slots = (yy(0), yy(4))
     for i in range(2):
         xb[slots[i], pl.ds(xrow, xbk), pl.ds(cl, 128)] = xsb[pl.ds(xrow, xbk), i * 128 : (i + 1) * 128]
-    for k in range(1, nx):
+    for k in sorted(range(1, nx), key=lambda d: -min(d, nx - d)):
         to = pl.multiple_of(xx(k) * xbk, 16)
         for i in range(2):
             send(
@@ -247,6 +242,11 @@
                 xb.at[slots[i], pl.ds(xrow, xbk), pl.ds(cl, 128)],
                 xs.at[i, k], xr.at[i, k], dx=xx(k),
             )
+
+    ring(0, 0)
+    for k in range(1, nx):
+        rc(kv_ref, kvb.at[z, xx(-k)], kxs.at[k], kxr.at[k]).wait_recv()
+        ring(0, nx - k)
 
     rc(q_ref, qb.at[b * 2 + oc], qs.at[0], qr.at[0]).wait_recv()
     rc(q_ref, qb.at[(1 - b) * 2 + c], qs.at[1], qr.at[1]).wait_recv()
@@ -324,43 +324,55 @@
     for step in range(max(steps - 2, 0)):
         for zi in ring_wait(step):
             attend(zi)
-    for i in range(6):
-        arrive(i)
-    later = ring_wait(steps - 2) if steps > 1 else []
-
-    lwg.wait()
-    lwu.wait()
-    for i, r in enumerate((0, 4, 1, 5, 7, 3, 2, 6)):
+    def first_layer(r, fresh):
         s = yy(r)
         g = half(s, ocl)
         rc(g, g, ds.at[r], dr.at[r]).wait_recv()
         w0 = pl.multiple_of(s * 256, 256)
         gd = dot(xb[s], wg[pl.ds(w0, 256), :])
         ud = dot(xb[s], wu[pl.ds(w0, 256), :])
-        if i == 0:
+        if fresh:
             ga[...] = gd
             up[...] = ud
         else:
             ga[...] += gd
             up[...] += ud
+
+    lwg.wait()
+    lwu.wait()
+    first_layer(0, True)
+    first_layer(4, False)
+    coming = (0, 2, 1, 3, 4, 5)
+    for n, i in enumerate(coming):
+        arrive(i)
+        if n >= 1:
+            k, r = plan[coming[n - 1]]
+            first_layer((r - k + NY) % NY, False)
+    later = ring_wait(steps - 2) if steps > 1 else []
+    k, r = plan[coming[5]]
+    first_layer((r - k + NY) % NY, False)
     gate = ga[...]
     hid = (gate / (1.0 + jnp.exp(-gate)) * up[...]).astype(BF)
     for copy in lwd:
         copy.wait()
-    order = (4, 3, 5, 1, 7, 2, 6, 0)
-    for r in order:
-        tmp[r % 2] = dot(hid, wd[yy(r)])
-        own[r] = tmp[r % 2, :, pl.ds(cl, 128)]
-        pbuf[r] = tmp[r % 2, :, pl.ds(ocl, 128)].astype(BF)
-        send(pbuf.at[r], prx.at[r], es.at[r], er.at[r], dc=oc)
-
     def paired(r):
         rc(pbuf.at[r], prx.at[r], es.at[r], er.at[r]).wait_recv()
         return own[r] + prx[r].astype(F32)
 
-    for r, i, dest in ((4, 0, yy(0 - 2 * sgn)), (3, 1, yy(1)), (5, 2, yy(-1)), (1, 3, yy(1)), (7, 4, yy(-1))):
-        psb[r] = paired(r).astype(BF)
-        send(psb.at[r], rs.at[i], ms.at[i], mr.at[i], dy=dest)
+    order = (4, 3, 5, 1, 7, 2, 6, 0)
+    route = {4: (0, yy(0 - 2 * sgn)), 3: (1, yy(1)), 5: (2, yy(-1)), 1: (3, yy(1)), 7: (4, yy(-1))}
+    for n in range(8 + 2):
+        if n < 8:
+            r = order[n]
+            tmp[r % 2] = dot(hid, wd[yy(r)])
+            own[r] = tmp[r % 2, :, pl.ds(cl, 128)]
+            pbuf[r] = tmp[r % 2, :, pl.ds(ocl, 128)].astype(BF)
+            send(pbuf.at[r], prx.at[r], es.at[r], er.at[r], dc=oc)
+        if n >= 2 and order[n - 2] in route:
+            r = order[n - 2]
+            i, dest = route[r]
+            psb[r] = paired(r).astype(BF)
+            send(psb.at[r], rs.at[i], ms.at[i], mr.at[i], dy=dest)
 
     def got_rs(i):
         rc(psb.at[0], rs.at[i], ms.at[i], mr.at[i]).wait_recv()
@@ -368,10 +380,6 @@
 
     for zi in later:
         attend(zi)
-    for k in range(1, nx):
-        g = wall.at[xx(-k), c]
-        rc(g, g, wxs.at[k], wxr.at[k]).wait_recv()
-        send(g, g, wds.at[k], wdr.at[k], dc=oc)
     far_sum = got_rs(0)
     right = c.astype(F32)
     psb[2] = (paired(2) + got_rs(1) + far_sum * right).astype(BF)
@@ -395,9 +403,13 @@
 
     ret[...] = (paired(0) + got_rs(3) + got_rs(4) + got_rs(5) + got_rs(6)).astype(BF)
     rbk[pl.ds(xrow, xbk), :] = ret[pl.ds(xrow, xbk), :]
-    for k in range(1, nx):
+    for k in sorted(range(1, nx), key=lambda d: -min(d, nx - d)):
         to = pl.multiple_of(xx(k) * xbk, 16)
         send(ret.at[pl.ds(to, xbk)], rbk.at[pl.ds(xrow, xbk)], vs.at[k], vr.at[k], dx=xx(k))
+    for k in range(1, nx):
+        g = wall.at[xx(-k), c]
+        rc(g, g, wxs.at[k], wxr.at[k]).wait_recv()
+        send(g, g, wds.at[k], wdr.at[k], dc=oc)
     for i, dy, dc, mm in members:
         rc(ob.at[pl.ds(0, 2)], orx.at[i], ts.at[i], tr.at[i]).wait_recv()
     heads = []
@@ -419,7 +431,7 @@
         rc(ret.at[pl.ds(0, xbk)], rbk.at[pl.ds(frm, xbk)], vs.at[k], vr.at[k]).wait_recv()
     t2[...] = dot(pb_ref[...], rbk[...]).astype(BF)
     fin[pl.ds(zrow, zb), :] = t2[pl.ds(zrow, zb), :]
-    for k in range(1, nz):
+    for k in sorted(range(1, nz), key=lambda d: -min(d, nz - d)):
         to = pl.multiple_of(zz(k) * zb, 16)
         send(t2.at[pl.ds(to, zb)], fin.at[pl.ds(zrow, zb)], us.at[k], ur.at[k], dz=zz(k))
 

time: 76.6 us -> 76 us (level)
  the two profiles are of different devices: /device:TPU:16 before, /device:TPU:1 now
where the time goes in v5:
time: 76 us; the launch traced here: 74.9 us
  Pallas kernels  72 us (95%)
  local copies, waits for them, and re-layouts  2.19 us (3%)
    pallas_call x1, Pallas kernels, call(): pl.pallas_call(functools.partial(kernel, nz, nx, cap), out_shape=(jax.Sha...  72 us
    unnamed x4, local copies, waits for them, and re-layouts  2.19 us

profile of v5, /device:TPU:1, one launch (start us, length us, event | category | flops | bytes accessed | tf_op | source)
XLA Modules:
  0.0 74.9 jit_solution(9625664587835668387)
XLA Ops:
  0.6 72.0 %layer.1 = (bf16[32,2048]{1,0:T(8,128)(2,1)}, bf16[128,128]{1,0:T(8,128)(2,1)}) custom-call(f32[128,128]{1,0:T(8,128)} %constant.4.clone.tab_ref, f32[1,64]{1,0:T(1,128)} %bitcast.18, f32[1,64]{1,0:T(1,128)} %bitcast.19, s32[2,128]{1,0:T(2,128)} %bitcast.16, f32[2,128]{1,0:T(2,128)} %bitcast.17, s32[1,384]{1,0:T(1,128)} %constant.5.clone.src_ref, ...), custom_call_target="tpu_custom_call" | custom-call | tf_op jit(solution)/shard_map/layer/pallas_call | solution.py:494
  72.7 0.0 copy-start
  72.7 1.6 %copy.20 = bf16[32,2048]{1,0:T(8,128)(2,1)} copy(bf16[32,2048]{1,0:T(8,128)(2,1)} %get-tuple-element.4) | data formatting | bytes 262144
  74.2 0.0 copy-done
  74.3 0.6 copy.21
Async XLA Ops:
  72.7 1.6 %copy-start = (bf16[128,128]{1,0:T(8,128)(2,1)S(1)}, bf16[128,128]{1,0:T(8,128)(2,1)}, u32[]{:S(2)}) copy-start(bf16[128,128]{1,0:T(8,128)(2,1)} %get-tuple-element.5) | copy-start | bytes 98308

commit v6 on v5

--- a/solution.py
+++ b/solution.py
@@ -196,6 +196,15 @@
     for k in (1, 7, 2, 6, 3, 5, 4):
         send(wall.at[x, c, y], wall.at[x, c, y], wys.at[k], wyr.at[k], dy=yy(k))
 
+    def spread(k):
+        g = wall.at[x, c, yy(-k)]
+        if k:
+            rc(g, g, wys.at[k], wyr.at[k]).wait_recv()
+        for j in range(1, nx):
+            send(g, g, wxs.at[k, j], wxr.at[k, j], dx=xx(j))
+
+    spread(0)
+
     for j in range(8):
         qd[j] = jnp.zeros((128, 512), BF)
         acc[j] = jnp.zeros((ODIM, 256), F32)
@@ -243,6 +252,8 @@
                 xs.at[i, k], xr.at[i, k], dx=xx(k),
             )
 
+    for k in (1, 7, 2, 6):
+        spread(k)
     ring(0, 0)
     for k in range(1, nx):
         rc(kv_ref, kvb.at[z, xx(-k)], kxs.at[k], kxr.at[k]).wait_recv()
@@ -307,11 +318,8 @@
 
     swap(0)
     swap(4)
-    for k in range(1, NY):
-        g = wall.at[x, c, yy(-k)]
-        rc(g, g, wys.at[k], wyr.at[k]).wait_recv()
-    for k in range(1, nx):
-        send(wall.at[x, c], wall.at[x, c], wxs.at[k], wxr.at[k], dx=xx(k))
+    for k in (3, 5, 4):
+        spread(k)
     send(wall.at[x, c], wall.at[x, c], wds.at[0], wdr.at[0], dc=oc)
 
     def arrive(i):
@@ -407,8 +415,10 @@
         to = pl.multiple_of(xx(k) * xbk, 16)
         send(ret.at[pl.ds(to, xbk)], rbk.at[pl.ds(xrow, xbk)], vs.at[k], vr.at[k], dx=xx(k))
     for k in range(1, nx):
+        for j in range(NY):
+            g = wall.at[xx(-k), c, yy(-j)]
+            rc(g, g, wxs.at[j, k], wxr.at[j, k]).wait_recv()
         g = wall.at[xx(-k), c]
-        rc(g, g, wxs.at[k], wxr.at[k]).wait_recv()
         send(g, g, wds.at[k], wdr.at[k], dc=oc)
     for i, dy, dc, mm in members:
         rc(ob.at[pl.ds(0, 2)], orx.at[i], ts.at[i], tr.at[i]).wait_recv()
@@ -486,7 +496,7 @@
         wide(rows, 256), wide(rows, 256), wide(2, rows, 256), wide(NY, rows, 128), big(NY, rows, 128),
         big(NY, rows, 128), big(NY, rows, 128), big(7, rows, 128), big(rows, 128), big(rows, 128),
         big(rows, 128), big(rows, 128),
-        dma(17), dma(nx), dma(nx), dma(nz, nx), dma(nz, nx), dma(nz, nx), dma(nz, nx), dma(3), dma(3), dma(3), dma(3), dma(NY), dma(NY), dma(nx), dma(nx),
+        dma(17), dma(nx), dma(nx), dma(nz, nx), dma(nz, nx), dma(nz, nx), dma(nz, nx), dma(3), dma(3), dma(3), dma(3), dma(NY), dma(NY), dma(NY, nx), dma(NY, nx),
         dma(nx), dma(nx), dma(3), dma(3),
         dma(nz), dma(nz), dma(2, nx), dma(2, nx), dma(6), dma(6), dma(8), dma(8), dma(8), dma(8), dma(7), dma(7),
         dma(nx), dma(nx), dma(nz), dma(nz),

time: 76 us -> 76.6 us (level)
  no operation moved by 1% of the time
where the time goes in v6:
time: 76.6 us; the launch traced here: 75.3 us
  Pallas kernels  72.4 us (95%)
  local copies, waits for them, and re-layouts  2.19 us (3%)
    pallas_call x1, Pallas kernels, call(): pl.pallas_call(functools.partial(kernel, nz, nx, cap), out_shape=(jax.Sha...  72.4 us
    unnamed x4, local copies, waits for them, and re-layouts  2.19 us

profile of v6, /device:TPU:1, one launch (start us, length us, event | category | flops | bytes accessed | tf_op | source)
XLA Modules:
  0.0 75.3 jit_solution(16483399781823643772)
XLA Ops:
  0.6 72.4 %layer.1 = (bf16[32,2048]{1,0:T(8,128)(2,1)}, bf16[128,128]{1,0:T(8,128)(2,1)}) custom-call(f32[128,128]{1,0:T(8,128)} %constant.4.clone.tab_ref, f32[1,64]{1,0:T(1,128)} %bitcast.18, f32[1,64]{1,0:T(1,128)} %bitcast.19, s32[2,128]{1,0:T(2,128)} %bitcast.16, f32[2,128]{1,0:T(2,128)} %bitcast.17, s32[1,384]{1,0:T(1,128)} %constant.5.clone.src_ref, ...), custom_call_target="tpu_custom_call" | custom-call | tf_op jit(solution)/shard_map/layer/pallas_call | solution.py:504
  73.1 0.0 copy-start
  73.1 1.6 %copy.20 = bf16[32,2048]{1,0:T(8,128)(2,1)} copy(bf16[32,2048]{1,0:T(8,128)(2,1)} %get-tuple-element.4) | data formatting | bytes 262144
  74.6 0.0 copy-done
  74.6 0.6 copy.21
Async XLA Ops:
  73.1 1.6 %copy-start = (bf16[128,128]{1,0:T(8,128)(2,1)S(1)}, bf16[128,128]{1,0:T(8,128)(2,1)}, u32[]{:S(2)}) copy-start(bf16[128,128]{1,0:T(8,128)(2,1)} %get-tuple-element.5) | copy-start | bytes 98308

commit v7 on v6

--- a/solution.py
+++ b/solution.py
@@ -252,8 +252,6 @@
                 xs.at[i, k], xr.at[i, k], dx=xx(k),
             )
 
-    for k in (1, 7, 2, 6):
-        spread(k)
     ring(0, 0)
     for k in range(1, nx):
         rc(kv_ref, kvb.at[z, xx(-k)], kxs.at[k], kxr.at[k]).wait_recv()
@@ -293,6 +291,8 @@
             held = p
         acc[7] += dot(vals, held)
 
+    for k in (1, 7, 2, 6):
+        spread(k)
     attend(z)
 
     for k in range(1, nx):

time: 76.6 us -> 76.5 us (level); the launches traced: 75.3 us -> 76.3 us
  Pallas kernels: 72.4 us -> 73.5 us
    pallas_call x1, Pallas kernels: 72.4 us -> 73.5 us  [call(): pl.pallas_call(functools.partial(kernel, nz, nx, cap), out_shape=(jax.Sha...]
where the time goes in v7:
time: 76.5 us; the launch traced here: 76.3 us
  Pallas kernels  73.5 us (96%)
  local copies, waits for them, and re-layouts  2.19 us (3%)
    pallas_call x1, Pallas kernels, call(): pl.pallas_call(functools.partial(kernel, nz, nx, cap), out_shape=(jax.Sha...  73.5 us
    unnamed x4, local copies, waits for them, and re-layouts  2.19 us

profile of v7, /device:TPU:1, one launch (start us, length us, event | category | flops | bytes accessed | tf_op | source)
XLA Modules:
  0.0 76.3 jit_solution(7712386968210437712)
XLA Ops:
  0.6 73.5 %layer.1 = (bf16[32,2048]{1,0:T(8,128)(2,1)}, bf16[128,128]{1,0:T(8,128)(2,1)}) custom-call(f32[128,128]{1,0:T(8,128)} %constant.4.clone.tab_ref, f32[1,64]{1,0:T(1,128)} %bitcast.18, f32[1,64]{1,0:T(1,128)} %bitcast.19, s32[2,128]{1,0:T(2,128)} %bitcast.16, f32[2,128]{1,0:T(2,128)} %bitcast.17, s32[1,384]{1,0:T(1,128)} %constant.5.clone.src_ref, ...), custom_call_target="tpu_custom_call" | custom-call | tf_op jit(solution)/shard_map/layer/pallas_call | solution.py:504
  74.1 0.0 copy-start
  74.1 1.6 %copy.20 = bf16[32,2048]{1,0:T(8,128)(2,1)} copy(bf16[32,2048]{1,0:T(8,128)(2,1)} %get-tuple-element.4) | data formatting | bytes 262144
  75.7 0.0 copy-done
  75.7 0.6 copy.21
Async XLA Ops:
  74.1 1.6 %copy-start = (bf16[128,128]{1,0:T(8,128)(2,1)S(1)}, bf16[128,128]{1,0:T(8,128)(2,1)}, u32[]{:S(2)}) copy-start(bf16[128,128]{1,0:T(8,128)(2,1)} %get-tuple-element.5) | copy-start | bytes 98308
